TPU v7x, 32 devices: a whole 2x2x4 slice. The times are simulated.
32 devices in a mesh: ep: 8 (over z, x), tp: 4 (over y, core).
Axes of the slice: x: 2, y: 2, z: 4, core: 2. Of those that a mesh axis runs over, the one named last changes fastest.
Arguments:
- tokens: bfloat16 [6144, 2048], P(('ep', 'tp')), may hold values from -6 to 6
- routes: int32 [6144, 2], P(('ep', 'tp')), may hold values from 0 to 7, all different within a row; in each aligned block of 192 rows (0 to 191, 192 to 383, ...) at most 64 rows name the same one
- gates: float32 [6144, 2], P(('ep', 'tp')), may hold values from 0.3 to 2.2
- pre_gain: float32 [2048], replicated, may hold values from 0.1 to 1.9
- w_gate: bfloat16 [8, 2048, 512], P('ep'), may hold values from -0.125 to 0.125
- w_up: bfloat16 [8, 2048, 512], P('ep'), may hold values from -0.125 to 0.125
- w_down: bfloat16 [8, 512, 2048], P('ep'), may hold values from -0.25 to 0.25
- sh_gate: bfloat16 [2048, 512], P('tp'), may hold values from -0.125 to 0.125
- sh_up: bfloat16 [2048, 512], P('tp'), may hold values from -0.125 to 0.125
- sh_down: bfloat16 [512, 2048], P(None, 'tp'), may hold values from -0.25 to 0.25
- post_gain: float32 [2048], replicated, may hold values from 0.1 to 1.9
Outputs:
- mixed: bfloat16 [6144, 2048], P('ep', 'tp')
Inputs may be any that keep to these rules, and one draw needn't show every extreme that they name: `routes`: each token names 2 different experts; among the rows of one device no expert is named more than 64 times, a bound that some block reaches.
All inputs are finite; a program needn't handle non-finite values.
Results may differ from a plain program's by a relative error of at most 0.0075.
Values may be sent and summed in bfloat16 or wider, within the bound.
No kernel may reach another device: no remote copies, remote signals or barrier semaphores. Data moves between devices by JAX's collectives and lax.ppermute only.
A program may use at most 64 MiB of HBM per device.

v0:
```python
import functools

import jax
import jax.numpy as jnp
from jax import lax
from jax.experimental import pallas as pl
from jax.experimental.pallas import tpu as pltpu
from jax.sharding import PartitionSpec as P


TOPK = 2
LANES = 128
EPS = 1e-06
F32, BF16 = jnp.float32, jnp.bfloat16
VMEM = pl.BlockSpec(memory_space=pltpu.VMEM)
SMEM = pl.BlockSpec(memory_space=pltpu.SMEM)
HBM = pl.BlockSpec(memory_space=pltpu.HBM)


def dot(a, b):
    return jnp.dot(a, b, preferred_element_type=F32)


def silu(v):
    return v / (1.0 + jnp.exp(-v))


def pre_kernel(capacity, me_ref, tok_in, routes_in, gates_in, gain_in, normed_ref, meta_ref, *refs):
    *bufs, tok, routes_ref, gates_ref, gain_ref, held, arrival, sent = refs
    experts = len(bufs)
    fetches = [
        pltpu.make_async_copy(source, target, arrival.at[i])
        for i, (source, target) in enumerate(
            [(routes_in, routes_ref), (tok_in, tok), (gain_in, gain_ref), (gates_in, gates_ref)]
        )
    ]
    for fetch in fetches:
        fetch.start()
    rows = tok.shape[0]
    fetches[0].wait()
    padded = -(-experts // 16) * 16
    rel = jnp.bitwise_xor(routes_ref[...], me_ref[0])
    first, second = rel[0:1], rel[1:2]
    expert = lax.broadcasted_iota(jnp.int32, (padded, rows), 0)
    hit0, hit1 = (first == expert).astype(F32), (second == expert).astype(F32)
    above = (
        lax.broadcasted_iota(jnp.int32, (rows, rows), 0)
        < lax.broadcasted_iota(jnp.int32, (rows, rows), 1)
    ).astype(F32).astype(BF16)
    before0 = dot(hit0.astype(BF16), above)
    before1 = dot(hit1.astype(BF16), above) + jnp.sum(hit0, axis=1, keepdims=True)
    slot0 = jnp.sum(before0 * hit0, axis=0, keepdims=True).astype(jnp.int32)
    slot1 = jnp.sum(before1 * hit1, axis=0, keepdims=True).astype(jnp.int32)
    dest0, dest1 = first * capacity + slot0, second * capacity + slot1
    meta_ref[...] = jnp.zeros_like(meta_ref)
    meta_ref[0:1] = dest0.astype(F32)
    meta_ref[1:2] = dest1.astype(F32)
    for fetch in fetches[1:]:
        fetch.wait()
    meta_ref[2:4] = gates_ref[...]
    x = tok[...].astype(F32)
    scale = lax.rsqrt(jnp.mean(x * x, axis=1, keepdims=True) + EPS)
    normed = (x * scale * gain_ref[...]).astype(BF16)
    normed_ref[...] = normed
    copies = []
    half = experts // 2
    for group in (range(half, experts), range(half)):
        low = group[0] * capacity
        place = lax.broadcasted_iota(jnp.int32, (half * capacity, rows), 0) + low
        chosen = ((place == dest0) | (place == dest1)).astype(F32).astype(BF16)
        held[low : low + half * capacity] = dot(chosen, normed).astype(BF16)
        for j in group:
            copy = pltpu.make_async_copy(held.at[pl.ds(j * capacity, capacity)], bufs[j], sent.at[j])
            copy.start()
            copies.append(copy)
    for copy in copies:
        copy.wait()


def gated_kernel(*refs):
    parts, (gate_ref, up_ref), out_ref = refs[:-3], refs[-3:-1], refs[-1]
    rows = jnp.concatenate([part[...] for part in parts], axis=0)
    gate, up = dot(rows, gate_ref[0]), dot(rows, up_ref[0])
    out_ref[...] = (silu(gate) * up).astype(BF16)


def shared_kernel(count, tp_ref, normed_ref, *refs):
    gates, ups, out_ref = refs[:count], refs[count : 2 * count], refs[-1]
    depth = gates[0].shape[0]
    gate = up = None
    for m in range(count):
        at = pl.multiple_of(jnp.bitwise_xor(tp_ref[0], m) * depth, depth)
        part = normed_ref[:, pl.ds(at, depth)]
        g, u = dot(part, gates[m][...]), dot(part, ups[m][...])
        gate, up = (g, u) if m == 0 else (gate + g, up + u)
    out_ref[...] = (silu(gate) * up).astype(BF16)


def shared_out_kernel(*refs):
    parts, down_ref, out_ref = refs[:-2], refs[-2], refs[-1]
    rows = parts[0].shape[0]
    for m, part in enumerate(parts):
        out_ref[m * rows : (m + 1) * rows] = dot(part[...], down_ref[...]).astype(BF16)


def combine_kernel(sources, sizes, capacity, *refs):
    groups, experts = len(sizes), sum(sizes)
    hidden = refs[: sources * groups]
    downs = refs[sources * groups : sources * groups + experts]
    metas = refs[sources * groups + experts : sources * groups + experts + sources]
    shared_ref, comb_ref, squares_ref, result = refs[-4:]
    j = 0
    for g, size in enumerate(sizes):
        for low in range(0, size * capacity, capacity):
            rows = jnp.concatenate(
                [hidden[g * sources + m][low : low + capacity] for m in range(sources)], axis=0
            )
            out = dot(rows, downs[j][...]).astype(BF16)
            for m in range(sources):
                result[m, j * capacity : (j + 1) * capacity] = out[m * capacity : (m + 1) * capacity]
            j += 1
    tokens = metas[0].shape[1]
    place = lax.broadcasted_iota(jnp.int32, (experts * capacity, tokens), 0)
    for m in range(sources):
        meta = metas[m][...]
        routed = None
        for k in range(TOPK):
            chosen = (place == meta[k : k + 1].astype(jnp.int32)).astype(F32).astype(BF16)
            picked = lax.dot_general(
                chosen, result[m], (((0,), (0,)), ((), ())), preferred_element_type=F32
            )
            gate = jnp.broadcast_to(meta[TOPK + k : TOPK + k + 1], (LANES, tokens)).T[:, 0:1]
            routed = picked * gate if k == 0 else routed + picked * gate
        here = slice(m * tokens, (m + 1) * tokens)
        combined = routed.astype(BF16).astype(F32) + shared_ref[here].astype(F32)
        comb_ref[here] = combined
        total = jnp.sum(combined * combined, axis=1, keepdims=True)
        squares_ref[m : m + 1] = jnp.broadcast_to(total, (tokens, LANES)).T[0:1]


def final_kernel(width, tp_ref, comb_ref, gain_ref, *refs):
    squares, out_ref = refs[:-1], refs[-1]
    count = len(squares)
    tokens = comb_ref.shape[0] // count
    gain = gain_ref[...]
    for m in range(count):
        total = squares[0][m : m + 1]
        for d in range(1, count):
            total = total + squares[d][m ^ d : (m ^ d) + 1]
        scale = lax.rsqrt(total / width + EPS)
        column = jnp.broadcast_to(scale, (LANES, tokens)).T[:, 0:1]
        at = pl.multiple_of(jnp.bitwise_xor(tp_ref[0], m) * tokens, 64)
        values = comb_ref[m * tokens : (m + 1) * tokens] * column * gain
        out_ref[pl.ds(at, tokens)] = values.astype(BF16)


def flip(value, axis, mask):
    size = lax.axis_size(axis)
    return lax.ppermute(value, axis, [(i, i ^ mask) for i in range(size)])


def gather_all(value, axis, steps=True):
    size = lax.axis_size(axis)
    held = {0: value}
    if not steps:
        return [value] + [flip(value, axis, j) for j in range(1, size)]
    mask = size // 2
    while mask:
        for j in list(held):
            held[j ^ mask] = flip(held[j], axis, mask)
        mask //= 2
    return [held[j] for j in range(size)]


def shape(dims, kind):
    return jax.ShapeDtypeStruct(dims, kind)


def call(kernel, out_shape, in_specs, out_specs, flops, moved, limit, scratch_shapes=()):
    def run(*operands):
        return pl.pallas_call(
            kernel,
            out_shape=out_shape,
            in_specs=in_specs,
            out_specs=out_specs,
            scratch_shapes=scratch_shapes,
            compiler_params=pltpu.CompilerParams(vmem_limit_bytes=limit * 2**20),
            cost_estimate=pl.CostEstimate(
                flops=int(flops), bytes_accessed=int(moved), transcendentals=0
            ),
        )(*operands)

    return run


def expert_groups(experts):
    near, quarter = experts // 2, experts // 4
    return [range(near), range(near, near + quarter), range(near + quarter, experts)]


def folded(
    tokens, routes, gates, pre_gain, w_gate, w_up, w_down, sh_gate, sh_up, sh_down, post_gain, *, capacity
):
    rows, width = tokens.shape
    experts, sources = lax.axis_size("ep"), lax.axis_size("tp")
    inner, columns = w_down.shape[1], width // sources
    ep = lax.axis_index("ep").astype(jnp.int32).reshape(1)
    tp = lax.axis_index("tp").astype(jnp.int32).reshape(1)
    groups = expert_groups(experts)

    own_down = lax.dynamic_slice_in_dim(w_down[0], tp[0] * columns, columns, axis=1)
    downs = gather_all(own_down, "ep")

    normed, meta, *bufs = call(
        functools.partial(pre_kernel, capacity),
        [shape((rows, width), BF16), shape((8, rows), F32)] + [shape((capacity, width), BF16)] * experts,
        [SMEM] + [HBM] * 4,
        [VMEM, VMEM] + [HBM] * experts,
        2 * rows * experts * capacity * width,
        4 * rows * width,
        60,
        [
            pltpu.VMEM((rows, width), BF16),
            pltpu.VMEM((TOPK, rows), jnp.int32),
            pltpu.VMEM((TOPK, rows), F32),
            pltpu.VMEM((1, width), F32),
            pltpu.VMEM((experts * capacity, width), BF16),
            pltpu.SemaphoreType.DMA((4,)),
            pltpu.SemaphoreType.DMA((experts,)),
        ],
    )(ep, tokens, routes.T, gates.T, pre_gain.reshape(1, width))

    arrived = [bufs[0]] + [flip(bufs[j], "ep", j) for j in range(1, experts)]

    sh_gates, sh_ups = gather_all(sh_gate, "tp"), gather_all(sh_up, "tp")
    metas = gather_all(meta, "tp", steps=False)

    shared_hidden = call(
        functools.partial(shared_kernel, sources),
        shape((rows, sh_down.shape[0]), BF16),
        [SMEM] + [VMEM] * (1 + 2 * sources),
        VMEM,
        4 * rows * width * inner,
        4 * width * inner,
        16,
    )(tp, normed, *sh_gates, *sh_ups)
    shared = call(
        shared_out_kernel,
        shape((sources * rows, columns), BF16),
        [VMEM] * (sources + 1),
        VMEM,
        2 * sources * rows * inner * columns,
        2 * inner * columns,
        16,
    )(*gather_all(shared_hidden, "tp"), sh_down)

    hidden = []
    for g, blocks in enumerate(groups):
        size = len(blocks)
        out = call(
            gated_kernel,
            shape((size * capacity, inner), BF16),
            [VMEM] * (size + 2),
            VMEM,
            4 * size * capacity * width * inner,
            4 * width * inner,
            16,
        )(*[arrived[j] for j in blocks], w_gate, w_up)
        back = []
        for b, j in enumerate(blocks):
            block = out[b * capacity : (b + 1) * capacity]
            back.append(block if j == 0 else flip(block, "ep", j))
        hidden += gather_all(jnp.concatenate(back, axis=0), "tp", steps=g < len(groups) - 1)

    combined, squares = call(
        functools.partial(combine_kernel, sources, [len(blocks) for blocks in groups], capacity),
        [shape((sources * rows, columns), F32), shape((sources, rows), F32)],
        [VMEM] * (len(hidden) + experts + sources + 1),
        [VMEM] * 2,
        4 * sources * rows * experts * capacity * columns,
        2 * experts * inner * columns,
        24,
        [pltpu.VMEM((sources, experts * capacity, columns), BF16)],
    )(*hidden, *downs, *metas, shared)

    gain = lax.dynamic_slice_in_dim(post_gain, tp[0] * columns, columns).reshape(1, columns)
    return call(
        functools.partial(final_kernel, width),
        shape((sources * rows, columns), BF16),
        [SMEM] + [VMEM] * (2 + sources),
        VMEM,
        8 * sources * rows * columns,
        6 * sources * rows * columns,
        16,
    )(tp, combined, gain, *gather_all(squares, "tp", steps=False))


def plain(
    tokens, routes, gates, pre_gain, w_gate, w_up, w_down, sh_gate, sh_up, sh_down, post_gain, *, capacity
):
    tok_rows, full_width = tokens.shape
    experts_all = lax.axis_size("ep")
    inputs = tokens.astype(F32)
    scale_in = lax.rsqrt(jnp.mean(inputs * inputs, axis=1, keepdims=True) + EPS)
    normed = (inputs * scale_in * pre_gain[None, :]).astype(BF16)
    gate_shared = dot(normed, lax.all_gather(sh_gate, "tp", axis=0, tiled=True))
    up_shared = dot(normed, lax.all_gather(sh_up, "tp", axis=0, tiled=True))
    shared_hidden = (jax.nn.silu(gate_shared) * up_shared).astype(BF16)
    pair_count = tok_rows * TOPK
    expert_ids = routes.reshape(pair_count)
    matches = (expert_ids[:, None] == jnp.arange(experts_all, dtype=jnp.int32)[None, :]).astype(jnp.int32)
    earlier = jnp.cumsum(matches, axis=0) - matches
    dest_slot = expert_ids * capacity + jnp.sum(earlier * matches, axis=1)
    pair_token = jnp.arange(pair_count, dtype=jnp.int32) // TOPK
    slot_token = jnp.full((experts_all * capacity,), tok_rows, jnp.int32).at[dest_slot].set(pair_token)
    padded = jnp.concatenate([normed, jnp.zeros((1, full_width), BF16)], axis=0)
    outgoing = padded[slot_token].reshape(experts_all, capacity, full_width)
    arrived = lax.all_to_all(outgoing, "ep", split_axis=0, concat_axis=0, tiled=True)
    flat_rows = arrived.reshape(experts_all * capacity, full_width)
    hidden = (jax.nn.silu(dot(flat_rows, w_gate[0])) * dot(flat_rows, w_up[0])).astype(BF16)
    result = dot(hidden, w_down[0]).astype(BF16).reshape(arrived.shape)
    returned = lax.all_to_all(result, "ep", split_axis=0, concat_axis=0, tiled=True)
    picked = returned.reshape(experts_all * capacity, full_width)[dest_slot]
    weighted = picked.astype(F32) * gates.reshape(pair_count)[:, None]
    routed = jnp.sum(weighted.reshape(tok_rows, TOPK, full_width), axis=1).astype(BF16)
    shared = dot(shared_hidden, lax.all_gather(sh_down, "tp", axis=1, tiled=True)).astype(BF16)
    combined = routed.astype(F32) + shared.astype(F32)
    scale_out = lax.rsqrt(jnp.mean(combined * combined, axis=1, keepdims=True) + EPS)
    out_rows = (combined * scale_out * post_gain[None, :]).astype(BF16)
    return lax.all_to_all(out_rows, "tp", split_axis=1, concat_axis=0, tiled=True)


def folds(experts, sources):
    powers = experts & (experts - 1) == 0 and sources & (sources - 1) == 0
    return powers and experts >= 4 and sources >= 2


def per_device(tokens, *rest):
    experts, sources = lax.axis_size("ep"), lax.axis_size("tp")
    plan = folded if folds(experts, sources) else plain
    capacity = max(2, 4 * tokens.shape[0] * TOPK // (3 * experts))
    return plan(tokens, *rest, capacity=capacity)


def solution(mesh):
    return jax.shard_map(
        per_device,
        mesh=mesh,
        in_specs=(
            P(("ep", "tp"), None),
            P(("ep", "tp"), None),
            P(("ep", "tp"), None),
            P(),
            P("ep", None, None),
            P("ep", None, None),
            P("ep", None, None),
            P("tp", None),
            P("tp", None),
            P(None, "tp"),
            P(),
        ),
        out_specs=P("ep", "tp"),
        check_vma=False,
    )
```

profile of v0, /device:TPU:0, one launch (start us, length us, event | category | flops | bytes accessed | tf_op | source)
XLA Modules:
  0.0 185.3 jit_solution(17249497208376006852)
XLA Ops:
  0.0 4.3 %shard_map.109 = (bf16[192,2048]{1,0:T(8,128)(2,1)}, f32[8,192]{1,0:T(8,128)}, bf16[64,2048]{1,0:T(8,128)(2,1)}, bf16[64,2048]{1,0:T(8,128)(2,1)}, bf16[64,2048]...) custom-call(s32[1]{0:T(128)} %bitcast.1.me_ref, ...), custom_call_target="tpu_custom_call" | custom-call | flops 402653184 | bytes 1572864 | tf_op jit(solution)/shard_map/pallas_call | solution.py:181
  4.4 5.1 %collective-permute-start.16 = (bf16[64,2048]{1,0:T(8,128)(2,1)}, bf16[64,2048]{1,0:T(8,128)(2,1)S(1)}, u32[]{:S(2)}, u32[]{:S(2)}) collective-permute-start(bf16[64,2048]{1,0:T(8,128)(2,1)} %get-tuple-element.23), channel_id=1, source_target_pairs={{0,24},{4,28},{8,16},{12,20},{16,8},{20,12},{24,0},{28,4},{1,25},{... | collective-permute-start | bytes 786440 | tf_op jit(solution)/shard_map/ppermute | solution.py:159
  9.5 1.2 collective-permute-start.17
  10.7 1.5 collective-permute-start.31
  12.7 4.3 %collective-permute-done.16.refs_0_ = bf16[64,2048]{1,0:T(8,128)(2,1)S(1)} collective-permute-done((bf16[64,2048]{1,0:T(8,128)(2,1)}, bf16[64,2048]{1,0:T(8,128)(2,1)S(1)}, u32[]{:S(2)}, u32[]{:S(2)}) %collective-permute-start.16) | collective-permute-done | bytes 262176 | tf_op jit(solution)/shard_map/ppermute | solution.py:159
  17.0 10.9 %collective-permute-start.1 = (bf16[64,2048]{1,0:T(8,128)(2,1)}, bf16[64,2048]{1,0:T(8,128)(2,1)S(1)}, u32[]{:S(2)}, u32[]{:S(2)}) collective-permute-start(bf16[64,2048]{1,0:T(8,128)(2,1)} %get-tuple-element.19), channel_id=1, source_target_pairs={{0,8},{4,12},{8,0},{12,4},{16,24},{20,28},{24,16},{28,20},{1,9},{5... | collective-permute-start | bytes 786440 | tf_op jit(solution)/shard_map/ppermute | solution.py:159
  27.9 5.6 %collective-permute-start.2 = (bf16[64,2048]{1,0:T(8,128)(2,1)}, bf16[64,2048]{1,0:T(8,128)(2,1)S(1)}, u32[]{:S(2)}, u32[]{:S(2)}) collective-permute-start(bf16[64,2048]{1,0:T(8,128)(2,1)} %get-tuple-element.20), channel_id=1, source_target_pairs={{0,12},{4,8},{8,4},{12,0},{16,28},{20,24},{24,20},{28,16},{1,13},{... | collective-permute-start | bytes 786440 | tf_op jit(solution)/shard_map/ppermute | solution.py:159
  33.5 1.6 copy-done.1
  35.1 1.6 copy-done.3
  37.6 1.0 collective-permute-start.10
  39.4 3.5 %collective-permute-start.9 = (bf16[64,2048]{1,0:T(8,128)(2,1)S(1)}, bf16[64,2048]{1,0:T(8,128)(2,1)S(1)}, u32[]{:S(2)}, u32[]{:S(2)}) collective-permute-start(bf16[64,2048]{1,0:T(8,128)(2,1)S(1)} %copy-done.20), channel_id=1, source_target_pairs={{0,16},{4,20},{8,24},{12,28},{16,0},{20,4},{24,8},{28,12},{1,17},{... | collective-permute-start | bytes 786440 | tf_op jit(solution)/shard_map/ppermute | solution.py:159
  42.8 1.2 shard_map.110
  44.7 14.7 %collective-permute-done.10.refs_1_ = bf16[64,2048]{1,0:T(8,128)(2,1)S(1)} collective-permute-done((bf16[64,2048]{1,0:T(8,128)(2,1)S(1)}, bf16[64,2048]{1,0:T(8,128)(2,1)S(1)}, u32[]{:S(2)}, u32[]{:S(2)}) %collective-permute-start.10) | collective-permute-done | bytes 262176 | tf_op jit(solution)/shard_map/ppermute | solution.py:159
  60.0 4.2 %collective-permute-done.9.refs_0_ = bf16[64,2048]{1,0:T(8,128)(2,1)S(1)} collective-permute-done((bf16[64,2048]{1,0:T(8,128)(2,1)S(1)}, bf16[64,2048]{1,0:T(8,128)(2,1)S(1)}, u32[]{:S(2)}, u32[]{:S(2)}) %collective-permute-start.9) | collective-permute-done | bytes 262176 | tf_op jit(solution)/shard_map/ppermute | solution.py:159
  64.1 2.3 %collective-permute-start.18 = (bf16[64,512]{1,0:T(8,128)(2,1)S(1)}, bf16[64,512]{1,0:T(8,128)(2,1)S(1)}, u32[]{:S(2)}, u32[]{:S(2)}) collective-permute-start(bf16[64,512]{1,0:T(8,128)(2,1)S(1)} %get-tuple-element.34), channel_id=1, source_target_pairs={{0,24},{4,28},{8,16},{12,20},{16,8},{20,12},{24,0},{28,4},{1,25},{... | collective-permute-start | bytes 196616 | tf_op jit(solution)/shard_map/ppermute | solution.py:159
  67.2 3.0 %collective-permute-done.18 = bf16[64,512]{1,0:T(8,128)(2,1)S(1)} collective-permute-done((bf16[64,512]{1,0:T(8,128)(2,1)S(1)}, bf16[64,512]{1,0:T(8,128)(2,1)S(1)}, u32[]{:S(2)}, u32[]{:S(2)}) %collective-permute-start.18) | collective-permute-done | bytes 65568 | tf_op jit(solution)/shard_map/ppermute | solution.py:159
  70.8 4.6 %collective-permute-done.11 = bf16[64,512]{1,0:T(8,128)(2,1)S(1)} collective-permute-done((bf16[64,512]{1,0:T(8,128)(2,1)S(1)}, bf16[64,512]{1,0:T(8,128)(2,1)S(1)}, u32[]{:S(2)}, u32[]{:S(2)}) %collective-permute-start.11) | collective-permute-done | bytes 65568 | tf_op jit(solution)/shard_map/ppermute | solution.py:159
  75.4 3.8 %collective-permute-start.19 = (bf16[64,512]{1,0:T(8,128)(2,1)S(1)}, bf16[64,512]{1,0:T(8,128)(2,1)S(1)}, u32[]{:S(2)}, u32[]{:S(2)}) collective-permute-start(bf16[64,512]{1,0:T(8,128)(2,1)S(1)} %get-tuple-element.33), channel_id=1, source_target_pairs={{0,28},{4,24},{8,20},{12,16},{16,12},{20,8},{24,4},{28,0},{1,29},{... | collective-permute-start | bytes 196616 | tf_op jit(solution)/shard_map/ppermute | solution.py:159
  79.3 3.1 %collective-permute-done.19 = bf16[64,512]{1,0:T(8,128)(2,1)S(1)} collective-permute-done((bf16[64,512]{1,0:T(8,128)(2,1)S(1)}, bf16[64,512]{1,0:T(8,128)(2,1)S(1)}, u32[]{:S(2)}, u32[]{:S(2)}) %collective-permute-start.19) | collective-permute-done | bytes 65568 | tf_op jit(solution)/shard_map/ppermute | solution.py:159
  83.0 1.2 collective-permute-start.34
  84.3 4.3 %collective-permute-start.4 = (bf16[64,512]{1,0:T(8,128)(2,1)S(1)}, bf16[64,512]{1,0:T(8,128)(2,1)S(1)}, u32[]{:S(2)}, u32[]{:S(2)}) collective-permute-start(bf16[64,512]{1,0:T(8,128)(2,1)S(1)} %get-tuple-element.31), channel_id=1, source_target_pairs={{0,8},{4,12},{8,0},{12,4},{16,24},{20,28},{24,16},{28,20},{1,9},{5... | collective-permute-start | bytes 196616 | tf_op jit(solution)/shard_map/ppermute | solution.py:159
  89.2 1.2 collective-permute-start.21
  90.9 2.9 %collective-permute-done.5 = bf16[64,512]{1,0:T(8,128)(2,1)S(1)} collective-permute-done((bf16[64,512]{1,0:T(8,128)(2,1)S(1)}, bf16[64,512]{1,0:T(8,128)(2,1)S(1)}, u32[]{:S(2)}, u32[]{:S(2)}) %collective-permute-start.5) | collective-permute-done | bytes 65568 | tf_op jit(solution)/shard_map/ppermute | solution.py:159
  93.8 1.0 collective-permute-start.14
  95.4 1.1 collective-permute-start.37
  96.5 2.0 %collective-permute-done.21.refs_10_ = bf16[128,512]{1,0:T(8,128)(2,1)S(1)} collective-permute-done((bf16[128,512]{1,0:T(8,128)(2,1)}, bf16[128,512]{1,0:T(8,128)(2,1)S(1)}, u32[]{:S(2)}, u32[]{:S(2)}) %collective-permute-start.21) | collective-permute-done | bytes 131104 | tf_op jit(solution)/shard_map/ppermute | solution.py:159
  99.1 0.9 collective-permute-done.22.refs_11_
  100.0 1.1 collective-permute-start.33
  101.2 3.0 %collective-permute-done.14.refs_6_ = bf16[128,512]{1,0:T(8,128)(2,1)} collective-permute-done((bf16[128,512]{1,0:T(8,128)(2,1)S(1)}, bf16[128,512]{1,0:T(8,128)(2,1)}, u32[]{:S(2)}, u32[]{:S(2)}) %collective-permute-start.14) | collective-permute-done | bytes 131104 | tf_op jit(solution)/shard_map/ppermute | solution.py:159
  104.2 5.5 %collective-permute-start.26 = (bf16[512,512]{1,0:T(8,128)(2,1)S(1)}, bf16[512,512]{1,0:T(8,128)(2,1)S(1)}, u32[]{:S(2)}, u32[]{:S(2)}) collective-permute-start(bf16[512,512]{1,0:T(8,128)(2,1)S(1)} %dynamic-slice_bitcast_fusion.refs_12_), channel_id=1, source_target_pairs={{0,16},{4,20},{8,24},{12,28},{16,0},{20,4},{24,8},{28,12},{1,17},{... | collective-permute-start | bytes 1572872 | tf_op jit(solution)/shard_map/ppermute | solution.py:159
  110.0 3.6 %collective-permute-done.37.refs_6_ = bf16[512,512]{1,0:T(8,128)(2,1)} collective-permute-done((bf16[512,512]{1,0:T(8,128)(2,1)}, bf16[512,512]{1,0:T(8,128)(2,1)}, u32[]{:S(2)}, u32[]{:S(2)}) %collective-permute-start.37) | collective-permute-done | bytes 524320 | tf_op jit(solution)/shard_map/ppermute | solution.py:159
  113.6 3.2 %collective-permute-start.24 = (bf16[512,512]{1,0:T(8,128)(2,1)S(1)}, bf16[512,512]{1,0:T(8,128)(2,1)S(1)}, u32[]{:S(2)}, u32[]{:S(2)}) collective-permute-start(bf16[512,512]{1,0:T(8,128)(2,1)S(1)} %dynamic-slice_bitcast_fusion.refs_12_), channel_id=1, source_target_pairs={{0,8},{4,12},{8,0},{12,4},{16,24},{20,28},{24,16},{28,20},{1,9},{5... | collective-permute-start | bytes 1572872 | tf_op jit(solution)/shard_map/ppermute | solution.py:159
  117.4 16.4 %collective-permute-done.26.refs_16_ = bf16[512,512]{1,0:T(8,128)(2,1)S(1)} collective-permute-done((bf16[512,512]{1,0:T(8,128)(2,1)S(1)}, bf16[512,512]{1,0:T(8,128)(2,1)S(1)}, u32[]{:S(2)}, u32[]{:S(2)}) %collective-permute-start.26) | collective-permute-done | bytes 524320 | tf_op jit(solution)/shard_map/ppermute | solution.py:159
  133.7 1.0 pad_maximum_fusion.refs_0_
  134.7 1.6 collective-permute-start.7
  136.3 2.4 %shard_map.113.refs_0_ = bf16[192,512]{1,0:T(8,128)(2,1)S(1)} custom-call(s32[1]{0:T(128)} %bitcast.tp_ref, bf16[192,2048]{1,0:T(8,128)(2,1)S(1)} %copy-done.4, bf16[512,512]{1,0:T(8,128)(2,1)S(1)} %copy-done.6, bf16[512,512]{1,0:T(8,128)(2,1)S(1)} %collective-permute-done.33.refs_1_, bf16[512,512]{1,0:T(8,128)(2,1)} %collective-permute-done.34.refs_2_, ...), custom_call_target="tpu_custom_call" | custom-call | flops 805306368 | bytes 4194304 | tf_op jit(solution)/shard_map/pallas_call | solution.py:181
  139.0 1.5 collective-permute-start.40
  140.5 0.9 collective-permute-start.27
  141.3 2.4 %collective-permute-done.7.refs_2_ = bf16[256,512]{1,0:T(8,128)(2,1)S(1)} collective-permute-done((bf16[256,512]{1,0:T(8,128)(2,1)S(1)}, bf16[256,512]{1,0:T(8,128)(2,1)S(1)}, u32[]{:S(2)}, u32[]{:S(2)}) %collective-permute-start.7) | collective-permute-done | bytes 262176 | tf_op jit(solution)/shard_map/ppermute | solution.py:159
  143.7 6.3 %collective-permute-done.28.refs_18_ = bf16[512,512]{1,0:T(8,128)(2,1)S(1)} collective-permute-done((bf16[512,512]{1,0:T(8,128)(2,1)S(1)}, bf16[512,512]{1,0:T(8,128)(2,1)S(1)}, u32[]{:S(2)}, u32[]{:S(2)}) %collective-permute-start.28) | collective-permute-done | bytes 524320 | tf_op jit(solution)/shard_map/ppermute | solution.py:159
  151.1 0.9 collective-permute-done.39.refs_1_
  153.9 1.3 collective-permute-done.27.refs_17_
  155.3 11.2 %collective-permute-done.25.refs_15_ = bf16[512,512]{1,0:T(8,128)(2,1)S(1)} collective-permute-done((bf16[512,512]{1,0:T(8,128)(2,1)S(1)}, bf16[512,512]{1,0:T(8,128)(2,1)S(1)}, u32[]{:S(2)}, u32[]{:S(2)}) %collective-permute-start.25) | collective-permute-done | bytes 524320 | tf_op jit(solution)/shard_map/ppermute | solution.py:159
  166.5 9.7 %collective-permute-done.29.refs_19_ = bf16[512,512]{1,0:T(8,128)(2,1)S(1)} collective-permute-done((bf16[512,512]{1,0:T(8,128)(2,1)S(1)}, bf16[512,512]{1,0:T(8,128)(2,1)S(1)}, u32[]{:S(2)}, u32[]{:S(2)}) %collective-permute-start.29) | collective-permute-done | bytes 524320 | tf_op jit(solution)/shard_map/ppermute | solution.py:159
  176.2 3.5 %shard_map.115 = (f32[768,512]{1,0:T(8,128)S(1)}, f32[4,192]{1,0:T(4,128)S(1)}) custom-call(bf16[256,512]{1,0:T(8,128)(2,1)S(1)} %pad_maximum_fusion.refs_0_, bf16[256,512]{1,0:T(8,128)(2,1)S(1)} %collective-permute-done.6.refs_1_, bf16[256,512]{1,0:T(8,128)(2,1)S(1)} %collective-permute-done.7.refs_2_, bf16[256,512]{1,0:T(8,128)(2,1)S(1)} %collective-permute-done.8.refs_3_, ...), custom_call_target="tpu_custom_call" | custom-call | flops 805306368 | bytes 4194304 | tf_op jit(solution)/shard_map/pallas_call | solution.py:181
  179.8 1.2 collective-permute-start.43
  182.4 1.1 collective-permute-done.43.refs_2_
  184.1 1.2 shard_map.116
  (104 shorter events, 13.7 us)
Async XLA Ops:
  0.0 104.2 %copy-start = (bf16[1,512,2048]{2,1,0:T(8,128)(2,1)S(1)}, bf16[1,512,2048]{2,1,0:T(8,128)(2,1)}, u32[]{:S(2)}) copy-start(bf16[1,512,2048]{2,1,0:T(8,128)(2,1)} %param.17) | copy-start | bytes 6291460
  4.4 12.6 %collective-permute-start.16 = (bf16[64,2048]{1,0:T(8,128)(2,1)}, bf16[64,2048]{1,0:T(8,128)(2,1)S(1)}, u32[]{:S(2)}, u32[]{:S(2)}) collective-permute-start(bf16[64,2048]{1,0:T(8,128)(2,1)} %get-tuple-element.23), channel_id=1, source_target_pairs={{0,24},{4,28},{8,16},{12,20},{16,8},{20,12},{24,0},{28,4},{1,25},{... | collective-permute-start | bytes 786440 | tf_op jit(solution)/shard_map/ppermute | solution.py:159
  9.5 18.4 %collective-permute-start.17 = (bf16[64,2048]{1,0:T(8,128)(2,1)}, bf16[64,2048]{1,0:T(8,128)(2,1)S(1)}, u32[]{:S(2)}, u32[]{:S(2)}) collective-permute-start(bf16[64,2048]{1,0:T(8,128)(2,1)} %get-tuple-element.24), channel_id=1, source_target_pairs={{0,28},{4,24},{8,20},{12,16},{16,12},{20,8},{24,4},{28,0},{1,29},{... | collective-permute-start | bytes 786440 | tf_op jit(solution)/shard_map/ppermute | solution.py:159
  10.6 72.4 %collective-permute-start.30 = (f32[8,192]{1,0:T(8,128)}, f32[8,192]{1,0:T(8,128)S(1)}, u32[]{:S(2)}, u32[]{:S(2)}) collective-permute-start(f32[8,192]{1,0:T(8,128)} %get-tuple-element.25.refs_20_), channel_id=1, source_target_pairs={{0,1},{1,0},{2,3},{3,2},{4,5},{5,4},{6,7},{7,6},{8,9},{9,8},{10,11... | collective-permute-start | bytes 18440 | tf_op jit(solution)/shard_map/ppermute | solution.py:159
  10.7 73.6 %collective-permute-start.31 = (f32[8,192]{1,0:T(8,128)}, f32[8,192]{1,0:T(8,128)S(1)}, u32[]{:S(2)}, u32[]{:S(2)}) collective-permute-start(f32[8,192]{1,0:T(8,128)} %get-tuple-element.25.refs_20_), channel_id=1, source_target_pairs={{0,2},{1,3},{2,0},{3,1},{4,6},{5,7},{6,4},{7,5},{8,10},{9,11},{10,... | collective-permute-start | bytes 18440 | tf_op jit(solution)/shard_map/ppermute | solution.py:159
  12.2 25.3 %collective-permute-start = (bf16[64,2048]{1,0:T(8,128)(2,1)}, bf16[64,2048]{1,0:T(8,128)(2,1)S(1)}, u32[]{:S(2)}, u32[]{:S(2)}) collective-permute-start(bf16[64,2048]{1,0:T(8,128)(2,1)} %get-tuple-element.18), channel_id=1, source_target_pairs={{0,4},{4,0},{8,12},{12,8},{16,20},{20,16},{24,28},{28,24},{1,5},{5... | collective-permute-start | bytes 786440 | tf_op jit(solution)/shard_map/ppermute | solution.py:159
  17.0 20.6 %collective-permute-start.1 = (bf16[64,2048]{1,0:T(8,128)(2,1)}, bf16[64,2048]{1,0:T(8,128)(2,1)S(1)}, u32[]{:S(2)}, u32[]{:S(2)}) collective-permute-start(bf16[64,2048]{1,0:T(8,128)(2,1)} %get-tuple-element.19), channel_id=1, source_target_pairs={{0,8},{4,12},{8,0},{12,4},{16,24},{20,28},{24,16},{28,20},{1,9},{5... | collective-permute-start | bytes 786440 | tf_op jit(solution)/shard_map/ppermute | solution.py:159
  27.9 11.4 %collective-permute-start.2 = (bf16[64,2048]{1,0:T(8,128)(2,1)}, bf16[64,2048]{1,0:T(8,128)(2,1)S(1)}, u32[]{:S(2)}, u32[]{:S(2)}) collective-permute-start(bf16[64,2048]{1,0:T(8,128)(2,1)} %get-tuple-element.20), channel_id=1, source_target_pairs={{0,12},{4,8},{8,4},{12,0},{16,28},{20,24},{24,20},{28,16},{1,13},{... | collective-permute-start | bytes 786440 | tf_op jit(solution)/shard_map/ppermute | solution.py:159
  37.4 51.2 %collective-permute-start.32 = (f32[8,192]{1,0:T(8,128)S(1)}, f32[8,192]{1,0:T(8,128)S(1)}, u32[]{:S(2)}, u32[]{:S(2)}) collective-permute-start(f32[8,192]{1,0:T(8,128)S(1)} %copy-done.12), channel_id=1, source_target_pairs={{0,3},{1,2},{2,1},{3,0},{4,7},{5,6},{6,5},{7,4},{8,11},{9,10},{10,... | collective-permute-start | bytes 18440 | tf_op jit(solution)/shard_map/ppermute | solution.py:159
  37.6 21.8 %collective-permute-start.10 = (bf16[64,2048]{1,0:T(8,128)(2,1)S(1)}, bf16[64,2048]{1,0:T(8,128)(2,1)S(1)}, u32[]{:S(2)}, u32[]{:S(2)}) collective-permute-start(bf16[64,2048]{1,0:T(8,128)(2,1)S(1)} %copy-done.21), channel_id=1, source_target_pairs={{0,20},{4,16},{8,28},{12,24},{16,4},{20,0},{24,12},{28,8},{1,21},{... | collective-permute-start | bytes 786440 | tf_op jit(solution)/shard_map/ppermute | solution.py:159
  39.4 24.8 %collective-permute-start.9 = (bf16[64,2048]{1,0:T(8,128)(2,1)S(1)}, bf16[64,2048]{1,0:T(8,128)(2,1)S(1)}, u32[]{:S(2)}, u32[]{:S(2)}) collective-permute-start(bf16[64,2048]{1,0:T(8,128)(2,1)S(1)} %copy-done.20), channel_id=1, source_target_pairs={{0,16},{4,20},{8,24},{12,28},{16,0},{20,4},{24,8},{28,12},{1,17},{... | collective-permute-start | bytes 786440 | tf_op jit(solution)/shard_map/ppermute | solution.py:159
  59.4 29.2 %collective-permute-start.3 = (bf16[64,512]{1,0:T(8,128)(2,1)S(1)}, bf16[64,512]{1,0:T(8,128)(2,1)S(1)}, u32[]{:S(2)}, u32[]{:S(2)}) collective-permute-start(bf16[64,512]{1,0:T(8,128)(2,1)S(1)} %get-tuple-element.32), channel_id=1, source_target_pairs={{0,4},{4,0},{8,12},{12,8},{16,20},{20,16},{24,28},{28,24},{1,5},{5... | collective-permute-start | bytes 196616 | tf_op jit(solution)/shard_map/ppermute | solution.py:159
  64.1 6.1 %collective-permute-start.18 = (bf16[64,512]{1,0:T(8,128)(2,1)S(1)}, bf16[64,512]{1,0:T(8,128)(2,1)S(1)}, u32[]{:S(2)}, u32[]{:S(2)}) collective-permute-start(bf16[64,512]{1,0:T(8,128)(2,1)S(1)} %get-tuple-element.34), channel_id=1, source_target_pairs={{0,24},{4,28},{8,16},{12,20},{16,8},{20,12},{24,0},{28,4},{1,25},{... | collective-permute-start | bytes 196616 | tf_op jit(solution)/shard_map/ppermute | solution.py:159
  67.2 69.1 %copy-start.4 = (bf16[192,2048]{1,0:T(8,128)(2,1)S(1)}, bf16[192,2048]{1,0:T(8,128)(2,1)}, u32[]{:S(2)}) copy-start(bf16[192,2048]{1,0:T(8,128)(2,1)} %get-tuple-element.26.normed_ref) | copy-start | bytes 2359300
  70.2 5.2 %collective-permute-start.11 = (bf16[64,512]{1,0:T(8,128)(2,1)S(1)}, bf16[64,512]{1,0:T(8,128)(2,1)S(1)}, u32[]{:S(2)}, u32[]{:S(2)}) collective-permute-start(bf16[64,512]{1,0:T(8,128)(2,1)S(1)} %get-tuple-element.36), channel_id=1, source_target_pairs={{0,16},{4,20},{8,24},{12,28},{16,0},{20,4},{24,8},{28,12},{1,17},{... | collective-permute-start | bytes 196616 | tf_op jit(solution)/shard_map/ppermute | solution.py:159
  75.4 7.0 %collective-permute-start.19 = (bf16[64,512]{1,0:T(8,128)(2,1)S(1)}, bf16[64,512]{1,0:T(8,128)(2,1)S(1)}, u32[]{:S(2)}, u32[]{:S(2)}) collective-permute-start(bf16[64,512]{1,0:T(8,128)(2,1)S(1)} %get-tuple-element.33), channel_id=1, source_target_pairs={{0,28},{4,24},{8,20},{12,16},{16,12},{20,8},{24,4},{28,0},{1,29},{... | collective-permute-start | bytes 196616 | tf_op jit(solution)/shard_map/ppermute | solution.py:159
  82.4 6.8 %collective-permute-start.12 = (bf16[64,512]{1,0:T(8,128)(2,1)S(1)}, bf16[64,512]{1,0:T(8,128)(2,1)S(1)}, u32[]{:S(2)}, u32[]{:S(2)}) collective-permute-start(bf16[64,512]{1,0:T(8,128)(2,1)S(1)} %get-tuple-element.35), channel_id=1, source_target_pairs={{0,20},{4,16},{8,28},{12,24},{16,4},{20,0},{24,12},{28,8},{1,21},{... | collective-permute-start | bytes 196616 | tf_op jit(solution)/shard_map/ppermute | solution.py:159
  83.0 26.7 %collective-permute-start.34 = (bf16[512,512]{1,0:T(8,128)(2,1)S(1)}, bf16[512,512]{1,0:T(8,128)(2,1)}, u32[]{:S(2)}, u32[]{:S(2)}) collective-permute-start(bf16[512,512]{1,0:T(8,128)(2,1)S(1)} %copy-done.6), channel_id=1, source_target_pairs={{0,2},{1,3},{2,0},{3,1},{4,6},{5,7},{6,4},{7,5},{8,10},{9,11},{10,... | collective-permute-start | bytes 1572872 | tf_op jit(solution)/shard_map/ppermute | solution.py:159
  84.3 6.6 %collective-permute-start.4 = (bf16[64,512]{1,0:T(8,128)(2,1)S(1)}, bf16[64,512]{1,0:T(8,128)(2,1)S(1)}, u32[]{:S(2)}, u32[]{:S(2)}) collective-permute-start(bf16[64,512]{1,0:T(8,128)(2,1)S(1)} %get-tuple-element.31), channel_id=1, source_target_pairs={{0,8},{4,12},{8,0},{12,4},{16,24},{20,28},{24,16},{28,20},{1,9},{5... | collective-permute-start | bytes 196616 | tf_op jit(solution)/shard_map/ppermute | solution.py:159
  88.6 5.2 %collective-permute-start.5 = (bf16[64,512]{1,0:T(8,128)(2,1)S(1)}, bf16[64,512]{1,0:T(8,128)(2,1)S(1)}, u32[]{:S(2)}, u32[]{:S(2)}) collective-permute-start(bf16[64,512]{1,0:T(8,128)(2,1)S(1)} %get-tuple-element.30), channel_id=1, source_target_pairs={{0,12},{4,8},{8,4},{12,0},{16,28},{20,24},{24,20},{28,16},{1,13},{... | collective-permute-start | bytes 196616 | tf_op jit(solution)/shard_map/ppermute | solution.py:159
  88.7 6.1 %collective-permute-start.20 = (bf16[128,512]{1,0:T(8,128)(2,1)}, bf16[128,512]{1,0:T(8,128)(2,1)S(1)}, u32[]{:S(2)}, u32[]{:S(2)}) collective-permute-start(bf16[128,512]{1,0:T(8,128)(2,1)} %constant_dynamic-update-slice_fusion.2.refs_8_), channel_id=1, source_target_pairs={{0,1},{1,0},{2,3},{3,2},{4,5},{5,4},{6,7},{7,6},{8,9},{9,8},{10,11... | collective-permute-start | bytes 393224 | tf_op jit(solution)/shard_map/ppermute | solution.py:159
  89.2 9.3 %collective-permute-start.21 = (bf16[128,512]{1,0:T(8,128)(2,1)}, bf16[128,512]{1,0:T(8,128)(2,1)S(1)}, u32[]{:S(2)}, u32[]{:S(2)}) collective-permute-start(bf16[128,512]{1,0:T(8,128)(2,1)} %constant_dynamic-update-slice_fusion.2.refs_8_), channel_id=1, source_target_pairs={{0,2},{1,3},{2,0},{3,1},{4,6},{5,7},{6,4},{7,5},{8,10},{9,11},{10,... | collective-permute-start | bytes 393224 | tf_op jit(solution)/shard_map/ppermute | solution.py:159
  90.9 9.2 %collective-permute-start.22 = (bf16[128,512]{1,0:T(8,128)(2,1)}, bf16[128,512]{1,0:T(8,128)(2,1)}, u32[]{:S(2)}, u32[]{:S(2)}) collective-permute-start(bf16[128,512]{1,0:T(8,128)(2,1)} %constant_dynamic-update-slice_fusion.2.refs_8_), channel_id=1, source_target_pairs={{0,3},{1,2},{2,1},{3,0},{4,7},{5,6},{6,5},{7,4},{8,11},{9,10},{10,... | collective-permute-start | bytes 393224 | tf_op jit(solution)/shard_map/ppermute | solution.py:159
  93.8 10.4 %collective-permute-start.14 = (bf16[128,512]{1,0:T(8,128)(2,1)S(1)}, bf16[128,512]{1,0:T(8,128)(2,1)}, u32[]{:S(2)}, u32[]{:S(2)}) collective-permute-start(bf16[128,512]{1,0:T(8,128)(2,1)S(1)} %constant_dynamic-update-slice_fusion.refs_4_), channel_id=1, source_target_pairs={{0,2},{1,3},{2,0},{3,1},{4,6},{5,7},{6,4},{7,5},{8,10},{9,11},{10,... | collective-permute-start | bytes 393224 | tf_op jit(solution)/shard_map/ppermute | solution.py:159
  95.4 18.2 %collective-permute-start.37 = (bf16[512,512]{1,0:T(8,128)(2,1)}, bf16[512,512]{1,0:T(8,128)(2,1)}, u32[]{:S(2)}, u32[]{:S(2)}) collective-permute-start(bf16[512,512]{1,0:T(8,128)(2,1)} %refs_4_.4), channel_id=1, source_target_pairs={{0,2},{1,3},{2,0},{3,1},{4,6},{5,7},{6,4},{7,5},{8,10},{9,11},{10,... | collective-permute-start | bytes 1572872 | tf_op jit(solution)/shard_map/ppermute | solution.py:159
  99.1 5.1 %collective-permute-start.13 = (bf16[128,512]{1,0:T(8,128)(2,1)S(1)}, bf16[128,512]{1,0:T(8,128)(2,1)}, u32[]{:S(2)}, u32[]{:S(2)}) collective-permute-start(bf16[128,512]{1,0:T(8,128)(2,1)S(1)} %constant_dynamic-update-slice_fusion.refs_4_), channel_id=1, source_target_pairs={{0,1},{1,0},{2,3},{3,2},{4,5},{5,4},{6,7},{7,6},{8,9},{9,8},{10,11... | collective-permute-start | bytes 393224 | tf_op jit(solution)/shard_map/ppermute | solution.py:159
  100.0 13.6 %collective-permute-start.33 = (bf16[512,512]{1,0:T(8,128)(2,1)S(1)}, bf16[512,512]{1,0:T(8,128)(2,1)S(1)}, u32[]{:S(2)}, u32[]{:S(2)}) collective-permute-start(bf16[512,512]{1,0:T(8,128)(2,1)S(1)} %copy-done.6), channel_id=1, source_target_pairs={{0,1},{1,0},{2,3},{3,2},{4,5},{5,4},{6,7},{7,6},{8,9},{9,8},{10,11... | collective-permute-start | bytes 1572872 | tf_op jit(solution)/shard_map/ppermute | solution.py:159
  104.2 12.6 %collective-permute-start.36 = (bf16[512,512]{1,0:T(8,128)(2,1)}, bf16[512,512]{1,0:T(8,128)(2,1)S(1)}, u32[]{:S(2)}, u32[]{:S(2)}) collective-permute-start(bf16[512,512]{1,0:T(8,128)(2,1)} %refs_4_.4), channel_id=1, source_target_pairs={{0,1},{1,0},{2,3},{3,2},{4,5},{5,4},{6,7},{7,6},{8,9},{9,8},{10,11... | collective-permute-start | bytes 1572872 | tf_op jit(solution)/shard_map/ppermute | solution.py:159
  104.2 29.5 %collective-permute-start.26 = (bf16[512,512]{1,0:T(8,128)(2,1)S(1)}, bf16[512,512]{1,0:T(8,128)(2,1)S(1)}, u32[]{:S(2)}, u32[]{:S(2)}) collective-permute-start(bf16[512,512]{1,0:T(8,128)(2,1)S(1)} %dynamic-slice_bitcast_fusion.refs_12_), channel_id=1, source_target_pairs={{0,16},{4,20},{8,24},{12,28},{16,0},{20,4},{24,8},{28,12},{1,17},{... | collective-permute-start | bytes 1572872 | tf_op jit(solution)/shard_map/ppermute | solution.py:159
  109.8 24.9 %collective-permute-start.35 = (bf16[512,512]{1,0:T(8,128)(2,1)}, bf16[512,512]{1,0:T(8,128)(2,1)S(1)}, u32[]{:S(2)}, u32[]{:S(2)}) collective-permute-start(bf16[512,512]{1,0:T(8,128)(2,1)} %collective-permute-done.34.refs_2_), channel_id=1, source_target_pairs={{0,1},{1,0},{2,3},{3,2},{4,5},{5,4},{6,7},{7,6},{8,9},{9,8},{10,11... | collective-permute-start | bytes 1572872 | tf_op jit(solution)/shard_map/ppermute | solution.py:159
  113.6 22.7 %collective-permute-start.38 = (bf16[512,512]{1,0:T(8,128)(2,1)}, bf16[512,512]{1,0:T(8,128)(2,1)S(1)}, u32[]{:S(2)}, u32[]{:S(2)}) collective-permute-start(bf16[512,512]{1,0:T(8,128)(2,1)} %collective-permute-done.37.refs_6_), channel_id=1, source_target_pairs={{0,1},{1,0},{2,3},{3,2},{4,5},{5,4},{6,7},{7,6},{8,9},{9,8},{10,11... | collective-permute-start | bytes 1572872 | tf_op jit(solution)/shard_map/ppermute | solution.py:159
  113.6 25.4 %collective-permute-start.24 = (bf16[512,512]{1,0:T(8,128)(2,1)S(1)}, bf16[512,512]{1,0:T(8,128)(2,1)S(1)}, u32[]{:S(2)}, u32[]{:S(2)}) collective-permute-start(bf16[512,512]{1,0:T(8,128)(2,1)S(1)} %dynamic-slice_bitcast_fusion.refs_12_), channel_id=1, source_target_pairs={{0,8},{4,12},{8,0},{12,4},{16,24},{20,28},{24,16},{28,20},{1,9},{5... | collective-permute-start | bytes 1572872 | tf_op jit(solution)/shard_map/ppermute | solution.py:159
  116.8 23.6 %collective-permute-start.23 = (bf16[512,512]{1,0:T(8,128)(2,1)S(1)}, bf16[512,512]{1,0:T(8,128)(2,1)S(1)}, u32[]{:S(2)}, u32[]{:S(2)}) collective-permute-start(bf16[512,512]{1,0:T(8,128)(2,1)S(1)} %dynamic-slice_bitcast_fusion.refs_12_), channel_id=1, source_target_pairs={{0,4},{4,0},{8,12},{12,8},{16,20},{20,16},{24,28},{28,24},{1,5},{5... | collective-permute-start | bytes 1572872 | tf_op jit(solution)/shard_map/ppermute | solution.py:159
  133.7 16.3 %collective-permute-start.28 = (bf16[512,512]{1,0:T(8,128)(2,1)S(1)}, bf16[512,512]{1,0:T(8,128)(2,1)S(1)}, u32[]{:S(2)}, u32[]{:S(2)}) collective-permute-start(bf16[512,512]{1,0:T(8,128)(2,1)S(1)} %collective-permute-done.26.refs_16_), channel_id=1, source_target_pairs={{0,8},{4,12},{8,0},{12,4},{16,24},{20,28},{24,16},{28,20},{1,9},{5... | collective-permute-start | bytes 1572872 | tf_op jit(solution)/shard_map/ppermute | solution.py:159
  134.7 9.0 %collective-permute-start.7 = (bf16[256,512]{1,0:T(8,128)(2,1)S(1)}, bf16[256,512]{1,0:T(8,128)(2,1)S(1)}, u32[]{:S(2)}, u32[]{:S(2)}) collective-permute-start(bf16[256,512]{1,0:T(8,128)(2,1)S(1)} %pad_maximum_fusion.refs_0_), channel_id=1, source_target_pairs={{0,2},{1,3},{2,0},{3,1},{4,6},{5,7},{6,4},{7,5},{8,10},{9,11},{10,... | collective-permute-start | bytes 786440 | tf_op jit(solution)/shard_map/ppermute | solution.py:159
  136.3 14.3 %collective-permute-start.6 = (bf16[256,512]{1,0:T(8,128)(2,1)S(1)}, bf16[256,512]{1,0:T(8,128)(2,1)S(1)}, u32[]{:S(2)}, u32[]{:S(2)}) collective-permute-start(bf16[256,512]{1,0:T(8,128)(2,1)S(1)} %pad_maximum_fusion.refs_0_), channel_id=1, source_target_pairs={{0,1},{1,0},{2,3},{3,2},{4,5},{5,4},{6,7},{7,6},{8,9},{9,8},{10,11... | collective-permute-start | bytes 786440 | tf_op jit(solution)/shard_map/ppermute | solution.py:159
  138.7 37.5 %copy-start.9 = (bf16[128,512]{1,0:T(8,128)(2,1)S(1)}, bf16[128,512]{1,0:T(8,128)(2,1)}, u32[]{:S(2)}) copy-start(bf16[128,512]{1,0:T(8,128)(2,1)} %copy-done.8) | copy-start | bytes 393220
  139.0 11.7 %collective-permute-start.40 = (bf16[192,512]{1,0:T(8,128)(2,1)S(1)}, bf16[192,512]{1,0:T(8,128)(2,1)S(1)}, u32[]{:S(2)}, u32[]{:S(2)}) collective-permute-start(bf16[192,512]{1,0:T(8,128)(2,1)S(1)} %shard_map.113.refs_0_), channel_id=1, source_target_pairs={{0,2},{1,3},{2,0},{3,1},{4,6},{5,7},{6,4},{7,5},{8,10},{9,11},{10,... | collective-permute-start | bytes 589832 | tf_op jit(solution)/shard_map/ppermute | solution.py:159
  140.5 14.8 %collective-permute-start.27 = (bf16[512,512]{1,0:T(8,128)(2,1)S(1)}, bf16[512,512]{1,0:T(8,128)(2,1)S(1)}, u32[]{:S(2)}, u32[]{:S(2)}) collective-permute-start(bf16[512,512]{1,0:T(8,128)(2,1)S(1)} %collective-permute-done.26.refs_16_), channel_id=1, source_target_pairs={{0,4},{4,0},{8,12},{12,8},{16,20},{20,16},{24,28},{28,24},{1,5},{5... | collective-permute-start | bytes 1572872 | tf_op jit(solution)/shard_map/ppermute | solution.py:159
  143.7 22.8 %collective-permute-start.25 = (bf16[512,512]{1,0:T(8,128)(2,1)S(1)}, bf16[512,512]{1,0:T(8,128)(2,1)S(1)}, u32[]{:S(2)}, u32[]{:S(2)}) collective-permute-start(bf16[512,512]{1,0:T(8,128)(2,1)S(1)} %collective-permute-done.24.refs_14_), channel_id=1, source_target_pairs={{0,4},{4,0},{8,12},{12,8},{16,20},{20,16},{24,28},{28,24},{1,5},{5... | collective-permute-start | bytes 1572872 | tf_op jit(solution)/shard_map/ppermute | solution.py:159
  150.0 26.2 %collective-permute-start.29 = (bf16[512,512]{1,0:T(8,128)(2,1)S(1)}, bf16[512,512]{1,0:T(8,128)(2,1)S(1)}, u32[]{:S(2)}, u32[]{:S(2)}) collective-permute-start(bf16[512,512]{1,0:T(8,128)(2,1)S(1)} %collective-permute-done.28.refs_18_), channel_id=1, source_target_pairs={{0,4},{4,0},{8,12},{12,8},{16,20},{20,16},{24,28},{28,24},{1,5},{5... | collective-permute-start | bytes 1572872 | tf_op jit(solution)/shard_map/ppermute | solution.py:159
  150.6 1.4 collective-permute-start.39
  150.6 1.7 collective-permute-start.41
  152.1 1.8 collective-permute-start.8
  152.4 1.6 collective-permute-start.15
  179.8 2.7 %collective-permute-start.42 = (f32[4,192]{1,0:T(4,128)S(1)}, f32[4,192]{1,0:T(4,128)S(1)}, u32[]{:S(2)}, u32[]{:S(2)}) collective-permute-start(f32[4,192]{1,0:T(4,128)S(1)} %get-tuple-element.28.refs_0_), channel_id=1, source_target_pairs={{0,1},{1,0},{2,3},{3,2},{4,5},{5,4},{6,7},{7,6},{8,9},{9,8},{10,11... | collective-permute-start | bytes 9224 | tf_op jit(solution)/shard_map/ppermute | solution.py:159
  179.8 3.7 %collective-permute-start.43 = (f32[4,192]{1,0:T(4,128)S(1)}, f32[4,192]{1,0:T(4,128)S(1)}, u32[]{:S(2)}, u32[]{:S(2)}) collective-permute-start(f32[4,192]{1,0:T(4,128)S(1)} %get-tuple-element.28.refs_0_), channel_id=1, source_target_pairs={{0,2},{1,3},{2,0},{3,1},{4,6},{5,7},{6,4},{7,5},{8,10},{9,11},{10,... | collective-permute-start | bytes 9224 | tf_op jit(solution)/shard_map/ppermute | solution.py:159
  181.1 3.0 %collective-permute-start.44 = (f32[4,192]{1,0:T(4,128)S(1)}, f32[4,192]{1,0:T(4,128)S(1)}, u32[]{:S(2)}, u32[]{:S(2)}) collective-permute-start(f32[4,192]{1,0:T(4,128)S(1)} %get-tuple-element.28.refs_0_), channel_id=1, source_target_pairs={{0,3},{1,2},{2,1},{3,0},{4,7},{5,6},{6,5},{7,4},{8,11},{9,10},{10,... | collective-permute-start | bytes 9224 | tf_op jit(solution)/shard_map/ppermute | solution.py:159
  (19 other events, 215.0 us)
where the time goes:
time: 186 us; the launch traced here: 185 us
  waiting for transfers between devices  99 us (53%)
  starting transfers between devices  63 us (34%)
  Pallas kernels  14.8 us (8%)
  local copies, waits for them, and re-layouts  7.35 us (4%)
    ppermute x45, waiting for transfers between devices, flip(): return lax.ppermute(value, axis, [(i, i ^ mask) for i in range(size)])  99 us
    ppermute x45, starting transfers between devices, flip(): return lax.ppermute(value, axis, [(i, i ^ mask) for i in range(size)])  63 us
    pallas_call x8, Pallas kernels, run(): pl.pallas_call(kernel, out_shape=out_shape, in_specs=in_specs, out_specs=...  14.8 us
    unnamed x46, local copies, waits for them, and re-layouts  5.26 us
  transfers between devices with their start and end apart: 45, of which 26 were waited for; matrix products, arithmetic and copies ran while one was open for 2% of the time, Pallas kernels for 3%

commit v1 on v0

--- a/solution.py
+++ b/solution.py
@@ -103,12 +103,11 @@
         out_ref[m * rows : (m + 1) * rows] = dot(part[...], down_ref[...]).astype(BF16)
 
 
-def combine_kernel(sources, sizes, capacity, *refs):
+def weighted(sources, sizes, first, capacity, refs, result, sums):
     groups, experts = len(sizes), sum(sizes)
     hidden = refs[: sources * groups]
     downs = refs[sources * groups : sources * groups + experts]
     metas = refs[sources * groups + experts : sources * groups + experts + sources]
-    shared_ref, comb_ref, squares_ref, result = refs[-4:]
     j = 0
     for g, size in enumerate(sizes):
         for low in range(0, size * capacity, capacity):
@@ -120,22 +119,33 @@
                 result[m, j * capacity : (j + 1) * capacity] = out[m * capacity : (m + 1) * capacity]
             j += 1
     tokens = metas[0].shape[1]
-    place = lax.broadcasted_iota(jnp.int32, (experts * capacity, tokens), 0)
+    place = lax.broadcasted_iota(jnp.int32, (experts * capacity, tokens), 0) + first * capacity
     for m in range(sources):
         meta = metas[m][...]
-        routed = None
+        total = None if sums is None else sums[m * tokens : (m + 1) * tokens]
         for k in range(TOPK):
             chosen = (place == meta[k : k + 1].astype(jnp.int32)).astype(F32).astype(BF16)
             picked = lax.dot_general(
                 chosen, result[m], (((0,), (0,)), ((), ())), preferred_element_type=F32
             )
             gate = jnp.broadcast_to(meta[TOPK + k : TOPK + k + 1], (LANES, tokens)).T[:, 0:1]
-            routed = picked * gate if k == 0 else routed + picked * gate
-        here = slice(m * tokens, (m + 1) * tokens)
-        combined = routed.astype(BF16).astype(F32) + shared_ref[here].astype(F32)
+            total = picked * gate if total is None else total + picked * gate
+        yield m, slice(m * tokens, (m + 1) * tokens), total
+
+
+def early_kernel(sources, sizes, capacity, *refs):
+    sums_ref, result = refs[-2:]
+    for _, here, total in weighted(sources, sizes, 0, capacity, refs, result, None):
+        sums_ref[here] = total
+
+
+def late_kernel(sources, sizes, first, capacity, *refs):
+    sums_ref, shared_ref, comb_ref, squares_ref, result = refs[-5:]
+    for m, here, total in weighted(sources, sizes, first, capacity, refs, result, sums_ref):
+        combined = total.astype(BF16).astype(F32) + shared_ref[here].astype(F32)
         comb_ref[here] = combined
-        total = jnp.sum(combined * combined, axis=1, keepdims=True)
-        squares_ref[m : m + 1] = jnp.broadcast_to(total, (tokens, LANES)).T[0:1]
+        squares = jnp.sum(combined * combined, axis=1, keepdims=True)
+        squares_ref[m : m + 1] = jnp.broadcast_to(squares, (combined.shape[0], LANES)).T[0:1]
 
 
 def final_kernel(width, tp_ref, comb_ref, gain_ref, *refs):
@@ -272,16 +282,35 @@
             back.append(block if j == 0 else flip(block, "ep", j))
         hidden += gather_all(jnp.concatenate(back, axis=0), "tp", steps=g < len(groups) - 1)
 
-    combined, squares = call(
-        functools.partial(combine_kernel, sources, [len(blocks) for blocks in groups], capacity),
-        [shape((sources * rows, columns), F32), shape((sources, rows), F32)],
-        [VMEM] * (len(hidden) + experts + sources + 1),
-        [VMEM] * 2,
-        4 * sources * rows * experts * capacity * columns,
-        2 * experts * inner * columns,
-        24,
-        [pltpu.VMEM((sources, experts * capacity, columns), BF16)],
-    )(*hidden, *downs, *metas, shared)
+    def weighing(kernel, sizes, first, outs, extra, *operands):
+        count = len(operands) - extra
+        slots = sum(sizes) * capacity
+        return call(
+            functools.partial(kernel, sources, sizes, *first, capacity),
+            outs,
+            [VMEM] * len(operands),
+            [VMEM] * len(outs),
+            4 * sources * rows * slots * columns,
+            2 * count * inner * columns,
+            24,
+            [pltpu.VMEM((sources, slots, columns), BF16)],
+        )(*operands)
+
+    sizes, last = [len(blocks) for blocks in groups], experts - len(groups[-1])
+    result = shape((sources * rows, columns), F32)
+    (sums,) = weighing(early_kernel, sizes[:-1], (), [result], 0, *hidden[:-sources], *downs[:last], *metas)
+    combined, squares = weighing(
+        late_kernel,
+        sizes[-1:],
+        (last,),
+        [result, shape((sources, rows), F32)],
+        2,
+        *hidden[-sources:],
+        *downs[last:],
+        *metas,
+        sums,
+        shared,
+    )
 
     gain = lax.dynamic_slice_in_dim(post_gain, tp[0] * columns, columns).reshape(1, columns)
     return call(

time: 186 us -> 182 us (0.978)
  waiting for transfers between devices: 99 us -> 116 us
  starting transfers between devices: 63 us -> 48.4 us
  local copies, waits for them, and re-layouts: 7.35 us -> 4.08 us
    ppermute x45, waiting for transfers between devices: 99 us -> 116 us  [flip(): return lax.ppermute(value, axis, [(i, i ^ mask) for i in range(size)])]
    ppermute x45, starting transfers between devices: 63 us -> 48.4 us  [flip(): return lax.ppermute(value, axis, [(i, i ^ mask) for i in range(size)])]
    unnamed x46 -> x26, local copies, waits for them, and re-layouts: 5.26 us -> 3.23 us
    pallas_call x8 -> x9, Pallas kernels: 14.8 us -> 13.6 us  [run(): pl.pallas_call(kernel, out_shape=out_shape, in_specs=in_specs, out_specs=...]
  transfers between devices with their start and end apart: 45 -> 45, of which waited for: 26 -> 19; matrix products, arithmetic and copies ran while one was open for 2% -> 0% of each run, Pallas kernels for 3% -> 3%
where the time goes in v1:
time: 182 us
  waiting for transfers between devices  116 us (64%)
  starting transfers between devices  48.4 us (27%)
  Pallas kernels  13.6 us (7%)
  local copies, waits for them, and re-layouts  4.08 us (2%)
    ppermute x45, waiting for transfers between devices, flip(): return lax.ppermute(value, axis, [(i, i ^ mask) for i in range(size)])  116 us
    ppermute x45, starting transfers between devices, flip(): return lax.ppermute(value, axis, [(i, i ^ mask) for i in range(size)])  48.4 us
    pallas_call x9, Pallas kernels, run(): pl.pallas_call(kernel, out_shape=out_shape, in_specs=in_specs, out_specs=...  13.6 us
  transfers between devices with their start and end apart: 45, of which 19 were waited for; matrix products, arithmetic and copies ran while one was open for 0% of the time, Pallas kernels for 3%

profile of v1, /device:TPU:0, one launch (start us, length us, event | category | flops | bytes accessed | tf_op | source)
XLA Modules:
  0.0 182.0 jit_solution(8080054216500509923)
XLA Ops:
  0.0 4.3 %shard_map.109 = (bf16[192,2048]{1,0:T(8,128)(2,1)}, f32[8,192]{1,0:T(8,128)}, bf16[64,2048]{1,0:T(8,128)(2,1)}, bf16[64,2048]{1,0:T(8,128)(2,1)}, bf16[64,2048]...) custom-call(s32[1]{0:T(128)} %bitcast.1.me_ref, ...), custom_call_target="tpu_custom_call" | custom-call | flops 402653184 | bytes 1572864 | tf_op jit(solution)/shard_map/pallas_call | solution.py:191
  4.3 4.1 %collective-permute-start.22 = (bf16[64,2048]{1,0:T(8,128)(2,1)}, bf16[64,2048]{1,0:T(8,128)(2,1)S(1)}, u32[]{:S(2)}, u32[]{:S(2)}) collective-permute-start(bf16[64,2048]{1,0:T(8,128)(2,1)} %get-tuple-element.24), channel_id=1, source_target_pairs={{0,16},{4,20},{8,24},{12,28},{16,0},{20,4},{24,8},{28,12},{1,17},{... | collective-permute-start | bytes 786440 | tf_op jit(solution)/shard_map/ppermute | solution.py:169
  8.5 1.3 collective-permute-start.23
  9.8 2.7 %collective-permute-start.7 = (bf16[512,512]{1,0:T(8,128)(2,1)S(1)}, bf16[512,512]{1,0:T(8,128)(2,1)S(1)}, u32[]{:S(2)}, u32[]{:S(2)}) collective-permute-start(bf16[512,512]{1,0:T(8,128)(2,1)S(1)} %dynamic-slice_bitcast_fusion.refs_8_), channel_id=1, source_target_pairs={{0,16},{4,20},{8,24},{12,28},{16,0},{20,4},{24,8},{28,12},{1,17},{... | collective-permute-start | bytes 1572872 | tf_op jit(solution)/shard_map/ppermute | solution.py:169
  12.4 1.6 collective-permute-start.30
  14.6 23.8 %collective-permute-done.22.refs_0_ = bf16[64,2048]{1,0:T(8,128)(2,1)S(1)} collective-permute-done((bf16[64,2048]{1,0:T(8,128)(2,1)}, bf16[64,2048]{1,0:T(8,128)(2,1)S(1)}, u32[]{:S(2)}, u32[]{:S(2)}) %collective-permute-start.22) | collective-permute-done | bytes 262176 | tf_op jit(solution)/shard_map/ppermute | solution.py:169
  38.4 6.9 %collective-permute-done.23.refs_1_ = bf16[64,2048]{1,0:T(8,128)(2,1)S(1)} collective-permute-done((bf16[64,2048]{1,0:T(8,128)(2,1)}, bf16[64,2048]{1,0:T(8,128)(2,1)S(1)}, u32[]{:S(2)}, u32[]{:S(2)}) %collective-permute-start.23) | collective-permute-done | bytes 262176 | tf_op jit(solution)/shard_map/ppermute | solution.py:169
  45.3 1.6 copy-done.1
  46.9 1.6 copy-done.3
  48.5 0.7 shard_map.112
  49.3 10.7 %collective-permute-done.14.refs_2_ = bf16[64,2048]{1,0:T(8,128)(2,1)S(1)} collective-permute-done((bf16[64,2048]{1,0:T(8,128)(2,1)}, bf16[64,2048]{1,0:T(8,128)(2,1)S(1)}, u32[]{:S(2)}, u32[]{:S(2)}) %collective-permute-start.14) | collective-permute-done | bytes 262176 | tf_op jit(solution)/shard_map/ppermute | solution.py:169
  60.0 3.5 %collective-permute-start = (bf16[64,2048]{1,0:T(8,128)(2,1)S(1)}, bf16[64,2048]{1,0:T(8,128)(2,1)S(1)}, u32[]{:S(2)}, u32[]{:S(2)}) collective-permute-start(bf16[64,2048]{1,0:T(8,128)(2,1)S(1)} %copy-done.11), channel_id=1, source_target_pairs={{0,24},{4,28},{8,16},{12,20},{16,8},{20,12},{24,0},{28,4},{1,25},{... | collective-permute-start | bytes 786440 | tf_op jit(solution)/shard_map/ppermute | solution.py:169
  63.6 8.6 %collective-permute-done.15.refs_3_ = bf16[64,2048]{1,0:T(8,128)(2,1)S(1)} collective-permute-done((bf16[64,2048]{1,0:T(8,128)(2,1)}, bf16[64,2048]{1,0:T(8,128)(2,1)S(1)}, u32[]{:S(2)}, u32[]{:S(2)}) %collective-permute-start.15) | collective-permute-done | bytes 262176 | tf_op jit(solution)/shard_map/ppermute | solution.py:169
  72.2 3.5 %collective-permute-start.1 = (bf16[64,2048]{1,0:T(8,128)(2,1)S(1)}, bf16[64,2048]{1,0:T(8,128)(2,1)S(1)}, u32[]{:S(2)}, u32[]{:S(2)}) collective-permute-start(bf16[64,2048]{1,0:T(8,128)(2,1)S(1)} %copy-done.10), channel_id=1, source_target_pairs={{0,28},{4,24},{8,20},{12,16},{16,12},{20,8},{24,4},{28,0},{1,29},{... | collective-permute-start | bytes 786440 | tf_op jit(solution)/shard_map/ppermute | solution.py:169
  75.6 1.2 shard_map.111
  76.9 1.6 collective-permute-start.11
  78.5 4.7 %collective-permute-done.1.refs_1_ = bf16[64,2048]{1,0:T(8,128)(2,1)S(1)} collective-permute-done((bf16[64,2048]{1,0:T(8,128)(2,1)S(1)}, bf16[64,2048]{1,0:T(8,128)(2,1)S(1)}, u32[]{:S(2)}, u32[]{:S(2)}) %collective-permute-start.1) | collective-permute-done | bytes 262176 | tf_op jit(solution)/shard_map/ppermute | solution.py:169
  83.2 4.5 %collective-permute-start.24 = (bf16[64,512]{1,0:T(8,128)(2,1)S(1)}, bf16[64,512]{1,0:T(8,128)(2,1)S(1)}, u32[]{:S(2)}, u32[]{:S(2)}) collective-permute-start(bf16[64,512]{1,0:T(8,128)(2,1)S(1)} %get-tuple-element.34), channel_id=1, source_target_pairs={{0,16},{4,20},{8,24},{12,28},{16,0},{20,4},{24,8},{28,12},{1,17},{... | collective-permute-start | bytes 196616 | tf_op jit(solution)/shard_map/ppermute | solution.py:169
  88.5 1.5 collective-permute-start.16
  90.3 3.5 %collective-permute-start.25 = (bf16[64,512]{1,0:T(8,128)(2,1)S(1)}, bf16[64,512]{1,0:T(8,128)(2,1)S(1)}, u32[]{:S(2)}, u32[]{:S(2)}) collective-permute-start(bf16[64,512]{1,0:T(8,128)(2,1)S(1)} %get-tuple-element.33), channel_id=1, source_target_pairs={{0,20},{4,16},{8,28},{12,24},{16,4},{20,0},{24,12},{28,8},{1,21},{... | collective-permute-start | bytes 196616 | tf_op jit(solution)/shard_map/ppermute | solution.py:169
  93.8 2.0 %collective-permute-start.18 = (bf16[64,512]{1,0:T(8,128)(2,1)S(1)}, bf16[64,512]{1,0:T(8,128)(2,1)S(1)}, u32[]{:S(2)}, u32[]{:S(2)}) collective-permute-start(bf16[64,512]{1,0:T(8,128)(2,1)S(1)} %get-tuple-element.30), channel_id=1, source_target_pairs={{0,12},{4,8},{8,4},{12,0},{16,28},{20,24},{24,20},{28,16},{1,13},{... | collective-permute-start | bytes 196616 | tf_op jit(solution)/shard_map/ppermute | solution.py:169
  95.9 1.9 %collective-permute-done.25 = bf16[64,512]{1,0:T(8,128)(2,1)S(1)} collective-permute-done((bf16[64,512]{1,0:T(8,128)(2,1)S(1)}, bf16[64,512]{1,0:T(8,128)(2,1)S(1)}, u32[]{:S(2)}, u32[]{:S(2)}) %collective-permute-start.25) | collective-permute-done | bytes 65568 | tf_op jit(solution)/shard_map/ppermute | solution.py:169
  97.8 0.8 collective-permute-start.2
  98.6 1.7 collective-permute-start.27
  100.3 3.3 %collective-permute-start.3 = (bf16[64,512]{1,0:T(8,128)(2,1)S(1)}, bf16[64,512]{1,0:T(8,128)(2,1)S(1)}, u32[]{:S(2)}, u32[]{:S(2)}) collective-permute-start(bf16[64,512]{1,0:T(8,128)(2,1)S(1)} %get-tuple-element.35), channel_id=1, source_target_pairs={{0,28},{4,24},{8,20},{12,16},{16,12},{20,8},{24,4},{28,0},{1,29},{... | collective-permute-start | bytes 196616 | tf_op jit(solution)/shard_map/ppermute | solution.py:169
  104.3 3.0 %collective-permute-done.3 = bf16[64,512]{1,0:T(8,128)(2,1)S(1)} collective-permute-done((bf16[64,512]{1,0:T(8,128)(2,1)S(1)}, bf16[64,512]{1,0:T(8,128)(2,1)S(1)}, u32[]{:S(2)}, u32[]{:S(2)}) %collective-permute-start.3) | collective-permute-done | bytes 65568 | tf_op jit(solution)/shard_map/ppermute | solution.py:169
  107.8 1.5 collective-permute-start.37
  110.3 11.8 %collective-permute-done.34.refs_2_ = bf16[512,512]{1,0:T(8,128)(2,1)S(1)} collective-permute-done((bf16[512,512]{1,0:T(8,128)(2,1)S(1)}, bf16[512,512]{1,0:T(8,128)(2,1)S(1)}, u32[]{:S(2)}, u32[]{:S(2)}) %collective-permute-start.34) | collective-permute-done | bytes 524320 | tf_op jit(solution)/shard_map/ppermute | solution.py:169
  122.1 7.8 %collective-permute-done.37.refs_6_ = bf16[512,512]{1,0:T(8,128)(2,1)S(1)} collective-permute-done((bf16[512,512]{1,0:T(8,128)(2,1)S(1)}, bf16[512,512]{1,0:T(8,128)(2,1)S(1)}, u32[]{:S(2)}, u32[]{:S(2)}) %collective-permute-start.37) | collective-permute-done | bytes 524320 | tf_op jit(solution)/shard_map/ppermute | solution.py:169
  129.9 1.0 collective-permute-start.8
  131.4 8.0 %collective-permute-done.20.refs_2_ = bf16[256,512]{1,0:T(8,128)(2,1)S(1)} collective-permute-done((bf16[256,512]{1,0:T(8,128)(2,1)S(1)}, bf16[256,512]{1,0:T(8,128)(2,1)S(1)}, u32[]{:S(2)}, u32[]{:S(2)}) %collective-permute-start.20) | collective-permute-done | bytes 262176 | tf_op jit(solution)/shard_map/ppermute | solution.py:169
  139.4 0.8 collective-permute-start.32
  140.3 1.2 collective-permute-start.31
  142.0 2.2 %collective-permute-done.8.refs_4_ = bf16[512,512]{1,0:T(8,128)(2,1)S(1)} collective-permute-done((bf16[512,512]{1,0:T(8,128)(2,1)S(1)}, bf16[512,512]{1,0:T(8,128)(2,1)S(1)}, u32[]{:S(2)}, u32[]{:S(2)}) %collective-permute-start.8) | collective-permute-done | bytes 524320 | tf_op jit(solution)/shard_map/ppermute | solution.py:169
  144.2 1.0 collective-permute-start.9
  145.2 1.0 shard_map.114.refs_0_
  146.3 1.6 collective-permute-start.40
  147.9 4.6 %collective-permute-done.40.refs_2_ = bf16[192,512]{1,0:T(8,128)(2,1)S(1)} collective-permute-done((bf16[192,512]{1,0:T(8,128)(2,1)S(1)}, bf16[192,512]{1,0:T(8,128)(2,1)S(1)}, u32[]{:S(2)}, u32[]{:S(2)}) %collective-permute-start.40) | collective-permute-done | bytes 196640 | tf_op jit(solution)/shard_map/ppermute | solution.py:169
  152.5 1.7 collective-permute-done.32.refs_13_
  154.2 11.2 %collective-permute-done.31.refs_11_ = bf16[512,512]{1,0:T(8,128)(2,1)S(1)} collective-permute-done((bf16[512,512]{1,0:T(8,128)(2,1)S(1)}, bf16[512,512]{1,0:T(8,128)(2,1)S(1)}, u32[]{:S(2)}, u32[]{:S(2)}) %collective-permute-start.31) | collective-permute-done | bytes 524320 | tf_op jit(solution)/shard_map/ppermute | solution.py:169
  165.9 1.8 %shard_map.113.refs_10_ = f32[768,512]{1,0:T(8,128)S(1)} custom-call(bf16[256,512]{1,0:T(8,128)(2,1)S(1)} %pad_maximum_fusion.refs_0_, bf16[256,512]{1,0:T(8,128)(2,1)S(1)} %collective-permute-done.19.refs_1_, bf16[256,512]{1,0:T(8,128)(2,1)S(1)} %collective-permute-done.20.refs_2_, bf16[256,512]{1,0:T(8,128)(2,1)S(1)} %collective-permute-done.21.refs_3_, ...), custom_call_target="tpu_custom_call" | custom-call | flops 603979776 | bytes 9437184 | tf_op jit(solution)/shard_map/pallas_call | solution.py:191
  168.4 3.3 %collective-permute-done.5.refs_2_ = bf16[128,512]{1,0:T(8,128)(2,1)S(1)} collective-permute-done((bf16[128,512]{1,0:T(8,128)(2,1)S(1)}, bf16[128,512]{1,0:T(8,128)(2,1)S(1)}, u32[]{:S(2)}, u32[]{:S(2)}) %collective-permute-start.5) | collective-permute-done | bytes 131104 | tf_op jit(solution)/shard_map/ppermute | solution.py:169
  171.7 3.4 %collective-permute-done.9.refs_5_ = bf16[512,512]{1,0:T(8,128)(2,1)S(1)} collective-permute-done((bf16[512,512]{1,0:T(8,128)(2,1)S(1)}, bf16[512,512]{1,0:T(8,128)(2,1)S(1)}, u32[]{:S(2)}, u32[]{:S(2)}) %collective-permute-start.9) | collective-permute-done | bytes 524320 | tf_op jit(solution)/shard_map/ppermute | solution.py:169
  175.1 1.9 %shard_map.116 = (f32[768,512]{1,0:T(8,128)S(1)}, f32[4,192]{1,0:T(4,128)S(1)}) custom-call(bf16[128,512]{1,0:T(8,128)(2,1)S(1)} %constant_dynamic-update-slice_fusion.refs_0_, bf16[128,512]{1,0:T(8,128)(2,1)S(1)} %collective-permute-done.4.refs_1_, bf16[128,512]{1,0:T(8,128)(2,1)S(1)} %collective-permute-done.5.refs_2_, ...), custom_call_target="tpu_custom_call" | custom-call | flops 201326592 | bytes 5242880 | tf_op jit(solution)/shard_map/pallas_call | solution.py:191
  177.7 1.2 collective-permute-start.44
  178.9 0.8 dynamic_slice.10
  179.7 1.1 collective-permute-done.43.refs_2_
  180.8 1.2 shard_map.117
  (85 shorter events, 6.9 us)
Async XLA Ops:
  4.3 34.0 %collective-permute-start.22 = (bf16[64,2048]{1,0:T(8,128)(2,1)}, bf16[64,2048]{1,0:T(8,128)(2,1)S(1)}, u32[]{:S(2)}, u32[]{:S(2)}) collective-permute-start(bf16[64,2048]{1,0:T(8,128)(2,1)} %get-tuple-element.24), channel_id=1, source_target_pairs={{0,16},{4,20},{8,24},{12,28},{16,0},{20,4},{24,8},{28,12},{1,17},{... | collective-permute-start | bytes 786440 | tf_op jit(solution)/shard_map/ppermute | solution.py:169
  8.5 36.8 %collective-permute-start.23 = (bf16[64,2048]{1,0:T(8,128)(2,1)}, bf16[64,2048]{1,0:T(8,128)(2,1)S(1)}, u32[]{:S(2)}, u32[]{:S(2)}) collective-permute-start(bf16[64,2048]{1,0:T(8,128)(2,1)} %get-tuple-element.25), channel_id=1, source_target_pairs={{0,20},{4,16},{8,28},{12,24},{16,4},{20,0},{24,12},{28,8},{1,21},{... | collective-permute-start | bytes 786440 | tf_op jit(solution)/shard_map/ppermute | solution.py:169
  9.8 100.0 %collective-permute-start.7 = (bf16[512,512]{1,0:T(8,128)(2,1)S(1)}, bf16[512,512]{1,0:T(8,128)(2,1)S(1)}, u32[]{:S(2)}, u32[]{:S(2)}) collective-permute-start(bf16[512,512]{1,0:T(8,128)(2,1)S(1)} %dynamic-slice_bitcast_fusion.refs_8_), channel_id=1, source_target_pairs={{0,16},{4,20},{8,24},{12,28},{16,0},{20,4},{24,8},{28,12},{1,17},{... | collective-permute-start | bytes 1572872 | tf_op jit(solution)/shard_map/ppermute | solution.py:169
  12.4 97.4 %collective-permute-start.30 = (bf16[512,512]{1,0:T(8,128)(2,1)S(1)}, bf16[512,512]{1,0:T(8,128)(2,1)S(1)}, u32[]{:S(2)}, u32[]{:S(2)}) collective-permute-start(bf16[512,512]{1,0:T(8,128)(2,1)S(1)} %dynamic-slice_bitcast_fusion.refs_8_), channel_id=1, source_target_pairs={{0,8},{4,12},{8,0},{12,4},{16,24},{20,28},{24,16},{28,20},{1,9},{5... | collective-permute-start | bytes 1572872 | tf_op jit(solution)/shard_map/ppermute | solution.py:169
  14.0 35.2 %collective-permute-start.13 = (bf16[64,2048]{1,0:T(8,128)(2,1)}, bf16[64,2048]{1,0:T(8,128)(2,1)S(1)}, u32[]{:S(2)}, u32[]{:S(2)}) collective-permute-start(bf16[64,2048]{1,0:T(8,128)(2,1)} %get-tuple-element.21), channel_id=1, source_target_pairs={{0,4},{4,0},{8,12},{12,8},{16,20},{20,16},{24,28},{28,24},{1,5},{5... | collective-permute-start | bytes 786440 | tf_op jit(solution)/shard_map/ppermute | solution.py:169
  38.3 21.7 %collective-permute-start.14 = (bf16[64,2048]{1,0:T(8,128)(2,1)}, bf16[64,2048]{1,0:T(8,128)(2,1)S(1)}, u32[]{:S(2)}, u32[]{:S(2)}) collective-permute-start(bf16[64,2048]{1,0:T(8,128)(2,1)} %get-tuple-element.22), channel_id=1, source_target_pairs={{0,8},{4,12},{8,0},{12,4},{16,24},{20,28},{24,16},{28,20},{1,9},{5... | collective-permute-start | bytes 786440 | tf_op jit(solution)/shard_map/ppermute | solution.py:169
  45.3 26.9 %collective-permute-start.15 = (bf16[64,2048]{1,0:T(8,128)(2,1)}, bf16[64,2048]{1,0:T(8,128)(2,1)S(1)}, u32[]{:S(2)}, u32[]{:S(2)}) collective-permute-start(bf16[64,2048]{1,0:T(8,128)(2,1)} %get-tuple-element.23), channel_id=1, source_target_pairs={{0,12},{4,8},{8,4},{12,0},{16,28},{20,24},{24,20},{28,16},{1,13},{... | collective-permute-start | bytes 786440 | tf_op jit(solution)/shard_map/ppermute | solution.py:169
  48.5 27.2 %copy-start.2 = (bf16[1,2048,512]{2,1,0:T(8,128)(2,1)S(1)}, bf16[1,2048,512]{2,1,0:T(8,128)(2,1)}, u32[]{:S(2)}) copy-start(bf16[1,2048,512]{2,1,0:T(8,128)(2,1)} %refs_2_.3) | copy-start | bytes 6291460
  48.5 27.1 %copy-start.8 = (bf16[64,2048]{1,0:T(8,128)(2,1)S(1)}, bf16[64,2048]{1,0:T(8,128)(2,1)}, u32[]{:S(2)}) copy-start(bf16[64,2048]{1,0:T(8,128)(2,1)} %get-tuple-element.20.refs_0_) | copy-start | bytes 786436
  49.2 39.2 %collective-permute-start.10 = (f32[8,192]{1,0:T(8,128)S(1)}, f32[8,192]{1,0:T(8,128)S(1)}, u32[]{:S(2)}, u32[]{:S(2)}) collective-permute-start(f32[8,192]{1,0:T(8,128)S(1)} %copy-done.9), channel_id=1, source_target_pairs={{0,1},{1,0},{2,3},{3,2},{4,5},{5,4},{6,7},{7,6},{8,9},{9,8},{10,11... | collective-permute-start | bytes 18440 | tf_op jit(solution)/shard_map/ppermute | solution.py:169
  60.0 16.9 %collective-permute-start = (bf16[64,2048]{1,0:T(8,128)(2,1)S(1)}, bf16[64,2048]{1,0:T(8,128)(2,1)S(1)}, u32[]{:S(2)}, u32[]{:S(2)}) collective-permute-start(bf16[64,2048]{1,0:T(8,128)(2,1)S(1)} %copy-done.11), channel_id=1, source_target_pairs={{0,24},{4,28},{8,16},{12,20},{16,8},{20,12},{24,0},{28,4},{1,25},{... | collective-permute-start | bytes 786440 | tf_op jit(solution)/shard_map/ppermute | solution.py:169
  72.2 11.0 %collective-permute-start.1 = (bf16[64,2048]{1,0:T(8,128)(2,1)S(1)}, bf16[64,2048]{1,0:T(8,128)(2,1)S(1)}, u32[]{:S(2)}, u32[]{:S(2)}) collective-permute-start(bf16[64,2048]{1,0:T(8,128)(2,1)S(1)} %copy-done.10), channel_id=1, source_target_pairs={{0,28},{4,24},{8,20},{12,16},{16,12},{20,8},{24,4},{28,0},{1,29},{... | collective-permute-start | bytes 786440 | tf_op jit(solution)/shard_map/ppermute | solution.py:169
  76.9 11.6 %collective-permute-start.11 = (f32[8,192]{1,0:T(8,128)S(1)}, f32[8,192]{1,0:T(8,128)S(1)}, u32[]{:S(2)}, u32[]{:S(2)}) collective-permute-start(f32[8,192]{1,0:T(8,128)S(1)} %copy-done.9), channel_id=1, source_target_pairs={{0,2},{1,3},{2,0},{3,1},{4,6},{5,7},{6,4},{7,5},{8,10},{9,11},{10,... | collective-permute-start | bytes 18440 | tf_op jit(solution)/shard_map/ppermute | solution.py:169
  83.2 62.0 %copy-start.4 = (bf16[192,2048]{1,0:T(8,128)(2,1)S(1)}, bf16[192,2048]{1,0:T(8,128)(2,1)}, u32[]{:S(2)}) copy-start(bf16[192,2048]{1,0:T(8,128)(2,1)} %get-tuple-element.26.normed_ref) | copy-start | bytes 2359300
  83.2 7.1 %collective-permute-start.24 = (bf16[64,512]{1,0:T(8,128)(2,1)S(1)}, bf16[64,512]{1,0:T(8,128)(2,1)S(1)}, u32[]{:S(2)}, u32[]{:S(2)}) collective-permute-start(bf16[64,512]{1,0:T(8,128)(2,1)S(1)} %get-tuple-element.34), channel_id=1, source_target_pairs={{0,16},{4,20},{8,24},{12,28},{16,0},{20,4},{24,8},{28,12},{1,17},{... | collective-permute-start | bytes 196616 | tf_op jit(solution)/shard_map/ppermute | solution.py:169
  88.4 5.3 %collective-permute-start.12 = (f32[8,192]{1,0:T(8,128)S(1)}, f32[8,192]{1,0:T(8,128)S(1)}, u32[]{:S(2)}, u32[]{:S(2)}) collective-permute-start(f32[8,192]{1,0:T(8,128)S(1)} %copy-done.9), channel_id=1, source_target_pairs={{0,3},{1,2},{2,1},{3,0},{4,7},{5,6},{6,5},{7,4},{8,11},{9,10},{10,... | collective-permute-start | bytes 18440 | tf_op jit(solution)/shard_map/ppermute | solution.py:169
  88.5 5.3 %collective-permute-start.16 = (bf16[64,512]{1,0:T(8,128)(2,1)S(1)}, bf16[64,512]{1,0:T(8,128)(2,1)S(1)}, u32[]{:S(2)}, u32[]{:S(2)}) collective-permute-start(bf16[64,512]{1,0:T(8,128)(2,1)S(1)} %get-tuple-element.32), channel_id=1, source_target_pairs={{0,4},{4,0},{8,12},{12,8},{16,20},{20,16},{24,28},{28,24},{1,5},{5... | collective-permute-start | bytes 196616 | tf_op jit(solution)/shard_map/ppermute | solution.py:169
  90.3 7.5 %collective-permute-start.25 = (bf16[64,512]{1,0:T(8,128)(2,1)S(1)}, bf16[64,512]{1,0:T(8,128)(2,1)S(1)}, u32[]{:S(2)}, u32[]{:S(2)}) collective-permute-start(bf16[64,512]{1,0:T(8,128)(2,1)S(1)} %get-tuple-element.33), channel_id=1, source_target_pairs={{0,20},{4,16},{8,28},{12,24},{16,4},{20,0},{24,12},{28,8},{1,21},{... | collective-permute-start | bytes 196616 | tf_op jit(solution)/shard_map/ppermute | solution.py:169
  93.8 4.9 %collective-permute-start.17 = (bf16[64,512]{1,0:T(8,128)(2,1)S(1)}, bf16[64,512]{1,0:T(8,128)(2,1)S(1)}, u32[]{:S(2)}, u32[]{:S(2)}) collective-permute-start(bf16[64,512]{1,0:T(8,128)(2,1)S(1)} %get-tuple-element.31), channel_id=1, source_target_pairs={{0,8},{4,12},{8,0},{12,4},{16,24},{20,28},{24,16},{28,20},{1,9},{5... | collective-permute-start | bytes 196616 | tf_op jit(solution)/shard_map/ppermute | solution.py:169
  93.8 6.5 %collective-permute-start.18 = (bf16[64,512]{1,0:T(8,128)(2,1)S(1)}, bf16[64,512]{1,0:T(8,128)(2,1)S(1)}, u32[]{:S(2)}, u32[]{:S(2)}) collective-permute-start(bf16[64,512]{1,0:T(8,128)(2,1)S(1)} %get-tuple-element.30), channel_id=1, source_target_pairs={{0,12},{4,8},{8,4},{12,0},{16,28},{20,24},{24,20},{28,16},{1,13},{... | collective-permute-start | bytes 196616 | tf_op jit(solution)/shard_map/ppermute | solution.py:169
  97.8 6.5 %collective-permute-start.2 = (bf16[64,512]{1,0:T(8,128)(2,1)S(1)}, bf16[64,512]{1,0:T(8,128)(2,1)S(1)}, u32[]{:S(2)}, u32[]{:S(2)}) collective-permute-start(bf16[64,512]{1,0:T(8,128)(2,1)S(1)} %get-tuple-element.36), channel_id=1, source_target_pairs={{0,24},{4,28},{8,16},{12,20},{16,8},{20,12},{24,0},{28,4},{1,25},{... | collective-permute-start | bytes 196616 | tf_op jit(solution)/shard_map/ppermute | solution.py:169
  98.6 9.2 %collective-permute-start.27 = (bf16[128,512]{1,0:T(8,128)(2,1)S(1)}, bf16[128,512]{1,0:T(8,128)(2,1)S(1)}, u32[]{:S(2)}, u32[]{:S(2)}) collective-permute-start(bf16[128,512]{1,0:T(8,128)(2,1)S(1)} %constant_dynamic-update-slice_fusion.2.refs_4_), channel_id=1, source_target_pairs={{0,2},{1,3},{2,0},{3,1},{4,6},{5,7},{6,4},{7,5},{8,10},{9,11},{10,... | collective-permute-start | bytes 393224 | tf_op jit(solution)/shard_map/ppermute | solution.py:169
  100.3 7.0 %collective-permute-start.3 = (bf16[64,512]{1,0:T(8,128)(2,1)S(1)}, bf16[64,512]{1,0:T(8,128)(2,1)S(1)}, u32[]{:S(2)}, u32[]{:S(2)}) collective-permute-start(bf16[64,512]{1,0:T(8,128)(2,1)S(1)} %get-tuple-element.35), channel_id=1, source_target_pairs={{0,28},{4,24},{8,20},{12,16},{16,12},{20,8},{24,4},{28,0},{1,29},{... | collective-permute-start | bytes 196616 | tf_op jit(solution)/shard_map/ppermute | solution.py:169
  104.3 5.0 %collective-permute-start.26 = (bf16[128,512]{1,0:T(8,128)(2,1)S(1)}, bf16[128,512]{1,0:T(8,128)(2,1)S(1)}, u32[]{:S(2)}, u32[]{:S(2)}) collective-permute-start(bf16[128,512]{1,0:T(8,128)(2,1)S(1)} %constant_dynamic-update-slice_fusion.2.refs_4_), channel_id=1, source_target_pairs={{0,1},{1,0},{2,3},{3,2},{4,5},{5,4},{6,7},{7,6},{8,9},{9,8},{10,11... | collective-permute-start | bytes 393224 | tf_op jit(solution)/shard_map/ppermute | solution.py:169
  107.3 14.8 %collective-permute-start.34 = (bf16[512,512]{1,0:T(8,128)(2,1)S(1)}, bf16[512,512]{1,0:T(8,128)(2,1)S(1)}, u32[]{:S(2)}, u32[]{:S(2)}) collective-permute-start(bf16[512,512]{1,0:T(8,128)(2,1)S(1)} %copy-done.6), channel_id=1, source_target_pairs={{0,2},{1,3},{2,0},{3,1},{4,6},{5,7},{6,4},{7,5},{8,10},{9,11},{10,... | collective-permute-start | bytes 1572872 | tf_op jit(solution)/shard_map/ppermute | solution.py:169
  107.8 22.1 %collective-permute-start.37 = (bf16[512,512]{1,0:T(8,128)(2,1)S(1)}, bf16[512,512]{1,0:T(8,128)(2,1)S(1)}, u32[]{:S(2)}, u32[]{:S(2)}) collective-permute-start(bf16[512,512]{1,0:T(8,128)(2,1)S(1)} %copy-done.7), channel_id=1, source_target_pairs={{0,2},{1,3},{2,0},{3,1},{4,6},{5,7},{6,4},{7,5},{8,10},{9,11},{10,... | collective-permute-start | bytes 1572872 | tf_op jit(solution)/shard_map/ppermute | solution.py:169
  109.3 20.6 %collective-permute-start.29 = (bf16[512,512]{1,0:T(8,128)(2,1)S(1)}, bf16[512,512]{1,0:T(8,128)(2,1)S(1)}, u32[]{:S(2)}, u32[]{:S(2)}) collective-permute-start(bf16[512,512]{1,0:T(8,128)(2,1)S(1)} %dynamic-slice_bitcast_fusion.refs_8_), channel_id=1, source_target_pairs={{0,4},{4,0},{8,12},{12,8},{16,20},{20,16},{24,28},{28,24},{1,5},{5... | collective-permute-start | bytes 1572872 | tf_op jit(solution)/shard_map/ppermute | solution.py:169
  109.8 21.1 %collective-permute-start.33 = (bf16[512,512]{1,0:T(8,128)(2,1)S(1)}, bf16[512,512]{1,0:T(8,128)(2,1)S(1)}, u32[]{:S(2)}, u32[]{:S(2)}) collective-permute-start(bf16[512,512]{1,0:T(8,128)(2,1)S(1)} %copy-done.6), channel_id=1, source_target_pairs={{0,1},{1,0},{2,3},{3,2},{4,5},{5,4},{6,7},{7,6},{8,9},{9,8},{10,11... | collective-permute-start | bytes 1572872 | tf_op jit(solution)/shard_map/ppermute | solution.py:169
  109.8 21.5 %collective-permute-start.36 = (bf16[512,512]{1,0:T(8,128)(2,1)S(1)}, bf16[512,512]{1,0:T(8,128)(2,1)S(1)}, u32[]{:S(2)}, u32[]{:S(2)}) collective-permute-start(bf16[512,512]{1,0:T(8,128)(2,1)S(1)} %copy-done.7), channel_id=1, source_target_pairs={{0,1},{1,0},{2,3},{3,2},{4,5},{5,4},{6,7},{7,6},{8,9},{9,8},{10,11... | collective-permute-start | bytes 1572872 | tf_op jit(solution)/shard_map/ppermute | solution.py:169
  122.1 19.4 %collective-permute-start.35 = (bf16[512,512]{1,0:T(8,128)(2,1)S(1)}, bf16[512,512]{1,0:T(8,128)(2,1)S(1)}, u32[]{:S(2)}, u32[]{:S(2)}) collective-permute-start(bf16[512,512]{1,0:T(8,128)(2,1)S(1)} %collective-permute-done.34.refs_2_), channel_id=1, source_target_pairs={{0,1},{1,0},{2,3},{3,2},{4,5},{5,4},{6,7},{7,6},{8,9},{9,8},{10,11... | collective-permute-start | bytes 1572872 | tf_op jit(solution)/shard_map/ppermute | solution.py:169
  129.9 11.6 %collective-permute-start.38 = (bf16[512,512]{1,0:T(8,128)(2,1)S(1)}, bf16[512,512]{1,0:T(8,128)(2,1)S(1)}, u32[]{:S(2)}, u32[]{:S(2)}) collective-permute-start(bf16[512,512]{1,0:T(8,128)(2,1)S(1)} %collective-permute-done.37.refs_6_), channel_id=1, source_target_pairs={{0,1},{1,0},{2,3},{3,2},{4,5},{5,4},{6,7},{7,6},{8,9},{9,8},{10,11... | collective-permute-start | bytes 1572872 | tf_op jit(solution)/shard_map/ppermute | solution.py:169
  129.9 14.3 %collective-permute-start.8 = (bf16[512,512]{1,0:T(8,128)(2,1)S(1)}, bf16[512,512]{1,0:T(8,128)(2,1)S(1)}, u32[]{:S(2)}, u32[]{:S(2)}) collective-permute-start(bf16[512,512]{1,0:T(8,128)(2,1)S(1)} %collective-permute-done.7.refs_12_), channel_id=1, source_target_pairs={{0,8},{4,12},{8,0},{12,4},{16,24},{20,28},{24,16},{28,20},{1,9},{5... | collective-permute-start | bytes 1572872 | tf_op jit(solution)/shard_map/ppermute | solution.py:169
  130.9 8.5 %collective-permute-start.20 = (bf16[256,512]{1,0:T(8,128)(2,1)S(1)}, bf16[256,512]{1,0:T(8,128)(2,1)S(1)}, u32[]{:S(2)}, u32[]{:S(2)}) collective-permute-start(bf16[256,512]{1,0:T(8,128)(2,1)S(1)} %pad_maximum_fusion.refs_0_), channel_id=1, source_target_pairs={{0,2},{1,3},{2,0},{3,1},{4,6},{5,7},{6,4},{7,5},{8,10},{9,11},{10,... | collective-permute-start | bytes 786440 | tf_op jit(solution)/shard_map/ppermute | solution.py:169
  131.3 9.0 %collective-permute-start.19 = (bf16[256,512]{1,0:T(8,128)(2,1)S(1)}, bf16[256,512]{1,0:T(8,128)(2,1)S(1)}, u32[]{:S(2)}, u32[]{:S(2)}) collective-permute-start(bf16[256,512]{1,0:T(8,128)(2,1)S(1)} %pad_maximum_fusion.refs_0_), channel_id=1, source_target_pairs={{0,1},{1,0},{2,3},{3,2},{4,5},{5,4},{6,7},{7,6},{8,9},{9,8},{10,11... | collective-permute-start | bytes 786440 | tf_op jit(solution)/shard_map/ppermute | solution.py:169
  139.4 14.8 %collective-permute-start.32 = (bf16[512,512]{1,0:T(8,128)(2,1)S(1)}, bf16[512,512]{1,0:T(8,128)(2,1)S(1)}, u32[]{:S(2)}, u32[]{:S(2)}) collective-permute-start(bf16[512,512]{1,0:T(8,128)(2,1)S(1)} %collective-permute-done.7.refs_12_), channel_id=1, source_target_pairs={{0,4},{4,0},{8,12},{12,8},{16,20},{20,16},{24,28},{28,24},{1,5},{5... | collective-permute-start | bytes 1572872 | tf_op jit(solution)/shard_map/ppermute | solution.py:169
  140.3 25.2 %collective-permute-start.31 = (bf16[512,512]{1,0:T(8,128)(2,1)S(1)}, bf16[512,512]{1,0:T(8,128)(2,1)S(1)}, u32[]{:S(2)}, u32[]{:S(2)}) collective-permute-start(bf16[512,512]{1,0:T(8,128)(2,1)S(1)} %collective-permute-done.30.refs_10_), channel_id=1, source_target_pairs={{0,4},{4,0},{8,12},{12,8},{16,20},{20,16},{24,28},{28,24},{1,5},{5... | collective-permute-start | bytes 1572872 | tf_op jit(solution)/shard_map/ppermute | solution.py:169
  141.5 6.4 %collective-permute-start.21 = (bf16[256,512]{1,0:T(8,128)(2,1)S(1)}, bf16[256,512]{1,0:T(8,128)(2,1)S(1)}, u32[]{:S(2)}, u32[]{:S(2)}) collective-permute-start(bf16[256,512]{1,0:T(8,128)(2,1)S(1)} %collective-permute-done.20.refs_2_), channel_id=1, source_target_pairs={{0,1},{1,0},{2,3},{3,2},{4,5},{5,4},{6,7},{7,6},{8,9},{9,8},{10,11... | collective-permute-start | bytes 786440 | tf_op jit(solution)/shard_map/ppermute | solution.py:169
  141.5 4.8 %collective-permute-start.28 = (bf16[128,512]{1,0:T(8,128)(2,1)S(1)}, bf16[128,512]{1,0:T(8,128)(2,1)S(1)}, u32[]{:S(2)}, u32[]{:S(2)}) collective-permute-start(bf16[128,512]{1,0:T(8,128)(2,1)S(1)} %collective-permute-done.27.refs_6_), channel_id=1, source_target_pairs={{0,1},{1,0},{2,3},{3,2},{4,5},{5,4},{6,7},{7,6},{8,9},{9,8},{10,11... | collective-permute-start | bytes 393224 | tf_op jit(solution)/shard_map/ppermute | solution.py:169
  144.2 30.9 %collective-permute-start.9 = (bf16[512,512]{1,0:T(8,128)(2,1)S(1)}, bf16[512,512]{1,0:T(8,128)(2,1)S(1)}, u32[]{:S(2)}, u32[]{:S(2)}) collective-permute-start(bf16[512,512]{1,0:T(8,128)(2,1)S(1)} %collective-permute-done.8.refs_4_), channel_id=1, source_target_pairs={{0,4},{4,0},{8,12},{12,8},{16,20},{20,16},{24,28},{28,24},{1,5},{5... | collective-permute-start | bytes 1572872 | tf_op jit(solution)/shard_map/ppermute | solution.py:169
  146.3 6.2 %collective-permute-start.40 = (bf16[192,512]{1,0:T(8,128)(2,1)S(1)}, bf16[192,512]{1,0:T(8,128)(2,1)S(1)}, u32[]{:S(2)}, u32[]{:S(2)}) collective-permute-start(bf16[192,512]{1,0:T(8,128)(2,1)S(1)} %shard_map.114.refs_0_), channel_id=1, source_target_pairs={{0,2},{1,3},{2,0},{3,1},{4,6},{5,7},{6,4},{7,5},{8,10},{9,11},{10,... | collective-permute-start | bytes 589832 | tf_op jit(solution)/shard_map/ppermute | solution.py:169
  147.9 18.0 %collective-permute-start.39 = (bf16[192,512]{1,0:T(8,128)(2,1)S(1)}, bf16[192,512]{1,0:T(8,128)(2,1)S(1)}, u32[]{:S(2)}, u32[]{:S(2)}) collective-permute-start(bf16[192,512]{1,0:T(8,128)(2,1)S(1)} %shard_map.114.refs_0_), channel_id=1, source_target_pairs={{0,1},{1,0},{2,3},{3,2},{4,5},{5,4},{6,7},{7,6},{8,9},{9,8},{10,11... | collective-permute-start | bytes 589832 | tf_op jit(solution)/shard_map/ppermute | solution.py:169
  152.5 15.3 %collective-permute-start.41 = (bf16[192,512]{1,0:T(8,128)(2,1)S(1)}, bf16[192,512]{1,0:T(8,128)(2,1)S(1)}, u32[]{:S(2)}, u32[]{:S(2)}) collective-permute-start(bf16[192,512]{1,0:T(8,128)(2,1)S(1)} %collective-permute-done.40.refs_2_), channel_id=1, source_target_pairs={{0,1},{1,0},{2,3},{3,2},{4,5},{5,4},{6,7},{7,6},{8,9},{9,8},{10,11... | collective-permute-start | bytes 589832 | tf_op jit(solution)/shard_map/ppermute | solution.py:169
  154.2 14.1 %collective-permute-start.4 = (bf16[128,512]{1,0:T(8,128)(2,1)S(1)}, bf16[128,512]{1,0:T(8,128)(2,1)S(1)}, u32[]{:S(2)}, u32[]{:S(2)}) collective-permute-start(bf16[128,512]{1,0:T(8,128)(2,1)S(1)} %constant_dynamic-update-slice_fusion.refs_0_), channel_id=1, source_target_pairs={{0,1},{1,0},{2,3},{3,2},{4,5},{5,4},{6,7},{7,6},{8,9},{9,8},{10,11... | collective-permute-start | bytes 393224 | tf_op jit(solution)/shard_map/ppermute | solution.py:169
  165.5 6.2 %collective-permute-start.5 = (bf16[128,512]{1,0:T(8,128)(2,1)S(1)}, bf16[128,512]{1,0:T(8,128)(2,1)S(1)}, u32[]{:S(2)}, u32[]{:S(2)}) collective-permute-start(bf16[128,512]{1,0:T(8,128)(2,1)S(1)} %constant_dynamic-update-slice_fusion.refs_0_), channel_id=1, source_target_pairs={{0,2},{1,3},{2,0},{3,1},{4,6},{5,7},{6,4},{7,5},{8,10},{9,11},{10,... | collective-permute-start | bytes 393224 | tf_op jit(solution)/shard_map/ppermute | solution.py:169
  165.9 5.8 %collective-permute-start.6 = (bf16[128,512]{1,0:T(8,128)(2,1)S(1)}, bf16[128,512]{1,0:T(8,128)(2,1)S(1)}, u32[]{:S(2)}, u32[]{:S(2)}) collective-permute-start(bf16[128,512]{1,0:T(8,128)(2,1)S(1)} %constant_dynamic-update-slice_fusion.refs_0_), channel_id=1, source_target_pairs={{0,3},{1,2},{2,1},{3,0},{4,7},{5,6},{6,5},{7,4},{8,11},{9,10},{10,... | collective-permute-start | bytes 393224 | tf_op jit(solution)/shard_map/ppermute | solution.py:169
  177.0 2.7 %collective-permute-start.42 = (f32[4,192]{1,0:T(4,128)S(1)}, f32[4,192]{1,0:T(4,128)S(1)}, u32[]{:S(2)}, u32[]{:S(2)}) collective-permute-start(f32[4,192]{1,0:T(4,128)S(1)} %get-tuple-element.28.refs_0_), channel_id=1, source_target_pairs={{0,1},{1,0},{2,3},{3,2},{4,5},{5,4},{6,7},{7,6},{8,9},{9,8},{10,11... | collective-permute-start | bytes 9224 | tf_op jit(solution)/shard_map/ppermute | solution.py:169
  177.1 3.7 %collective-permute-start.43 = (f32[4,192]{1,0:T(4,128)S(1)}, f32[4,192]{1,0:T(4,128)S(1)}, u32[]{:S(2)}, u32[]{:S(2)}) collective-permute-start(f32[4,192]{1,0:T(4,128)S(1)} %get-tuple-element.28.refs_0_), channel_id=1, source_target_pairs={{0,2},{1,3},{2,0},{3,1},{4,6},{5,7},{6,4},{7,5},{8,10},{9,11},{10,... | collective-permute-start | bytes 9224 | tf_op jit(solution)/shard_map/ppermute | solution.py:169
  177.7 3.1 %collective-permute-start.44 = (f32[4,192]{1,0:T(4,128)S(1)}, f32[4,192]{1,0:T(4,128)S(1)}, u32[]{:S(2)}, u32[]{:S(2)}) collective-permute-start(f32[4,192]{1,0:T(4,128)S(1)} %get-tuple-element.28.refs_0_), channel_id=1, source_target_pairs={{0,3},{1,2},{2,1},{3,0},{4,7},{5,6},{6,5},{7,4},{8,11},{9,10},{10,... | collective-permute-start | bytes 9224 | tf_op jit(solution)/shard_map/ppermute | solution.py:169
  (9 other events, 112.9 us)

commit v2 on v0

--- a/solution.py
+++ b/solution.py
@@ -103,55 +103,90 @@
         out_ref[m * rows : (m + 1) * rows] = dot(part[...], down_ref[...]).astype(BF16)
 
 
-def combine_kernel(sources, sizes, capacity, *refs):
+def column(row, rows):
+    return jnp.broadcast_to(row, (LANES, rows)).T[:, 0:1]
+
+
+def choices(meta, first, slots):
+    place = lax.broadcasted_iota(jnp.int32, (slots, meta.shape[1]), 0) + first
+    return [
+        (place == meta[k : k + 1].astype(jnp.int32)).astype(F32).astype(BF16) for k in range(TOPK)
+    ]
+
+
+def project(parts, down, result, at, capacity):
+    out = dot(jnp.concatenate(parts, axis=0), down).astype(BF16)
+    for m in range(len(parts)):
+        result[m, at : at + capacity] = out[m * capacity : (m + 1) * capacity]
+
+
+def weighted(chosen, meta, rows):
+    total = None
+    for k in range(TOPK):
+        picked = lax.dot_general(chosen[k], rows, (((0,), (0,)), ((), ())), preferred_element_type=F32)
+        term = picked * column(meta[TOPK + k : TOPK + k + 1], meta.shape[1])
+        total = term if total is None else total + term
+    return total
+
+
+def early_kernel(sources, sizes, capacity, *refs):
     groups, experts = len(sizes), sum(sizes)
     hidden = refs[: sources * groups]
     downs = refs[sources * groups : sources * groups + experts]
-    metas = refs[sources * groups + experts : sources * groups + experts + sources]
-    shared_ref, comb_ref, squares_ref, result = refs[-4:]
+    metas, sums_ref, result = refs[sources * groups + experts : -2], refs[-2], refs[-1]
     j = 0
     for g, size in enumerate(sizes):
         for low in range(0, size * capacity, capacity):
-            rows = jnp.concatenate(
-                [hidden[g * sources + m][low : low + capacity] for m in range(sources)], axis=0
-            )
-            out = dot(rows, downs[j][...]).astype(BF16)
-            for m in range(sources):
-                result[m, j * capacity : (j + 1) * capacity] = out[m * capacity : (m + 1) * capacity]
+            parts = [hidden[g * sources + m][low : low + capacity] for m in range(sources)]
+            project(parts, downs[j][...], result, j * capacity, capacity)
             j += 1
-    tokens = metas[0].shape[1]
-    place = lax.broadcasted_iota(jnp.int32, (experts * capacity, tokens), 0)
     for m in range(sources):
         meta = metas[m][...]
-        routed = None
-        for k in range(TOPK):
-            chosen = (place == meta[k : k + 1].astype(jnp.int32)).astype(F32).astype(BF16)
-            picked = lax.dot_general(
-                chosen, result[m], (((0,), (0,)), ((), ())), preferred_element_type=F32
-            )
-            gate = jnp.broadcast_to(meta[TOPK + k : TOPK + k + 1], (LANES, tokens)).T[:, 0:1]
-            routed = picked * gate if k == 0 else routed + picked * gate
+        tokens = meta.shape[1]
+        chosen = choices(meta, 0, experts * capacity)
+        sums_ref[m * tokens : (m + 1) * tokens] = weighted(chosen, meta, result[m])
+
+
+def late_kernel(sources, experts, first, capacity, *refs):
+    hidden, downs = refs[:sources], refs[sources : sources + experts]
+    metas, (shared_ref, sums_ref) = refs[sources + experts : -5], refs[-5:-3]
+    comb_ref, squares_ref, result = refs[-3:]
+    for j in range(experts):
+        at = j * capacity
+        project([part[at : at + capacity] for part in hidden], downs[j][...], result, at, capacity)
+    for m in range(sources):
+        meta = metas[m][...]
+        tokens = meta.shape[1]
         here = slice(m * tokens, (m + 1) * tokens)
+        chosen = choices(meta, first * capacity, experts * capacity)
+        routed = sums_ref[here] + weighted(chosen, meta, result[m])
         combined = routed.astype(BF16).astype(F32) + shared_ref[here].astype(F32)
         comb_ref[here] = combined
-        total = jnp.sum(combined * combined, axis=1, keepdims=True)
-        squares_ref[m : m + 1] = jnp.broadcast_to(total, (tokens, LANES)).T[0:1]
+        squares = jnp.sum(combined * combined, axis=1, keepdims=True)
+        squares_ref[m : m + 1] = jnp.broadcast_to(squares, (tokens, LANES)).T[0:1]
 
 
 def final_kernel(width, tp_ref, comb_ref, gain_ref, *refs):
-    squares, out_ref = refs[:-1], refs[-1]
+    *squares, out_ref, held, sent = refs
     count = len(squares)
     tokens = comb_ref.shape[0] // count
     gain = gain_ref[...]
+    copies = []
     for m in range(count):
         total = squares[0][m : m + 1]
         for d in range(1, count):
             total = total + squares[d][m ^ d : (m ^ d) + 1]
-        scale = lax.rsqrt(total / width + EPS)
-        column = jnp.broadcast_to(scale, (LANES, tokens)).T[:, 0:1]
+        scale = column(lax.rsqrt(total / width + EPS), tokens)
+        here = slice(m * tokens, (m + 1) * tokens)
+        held[here] = (comb_ref[here] * scale * gain).astype(BF16)
         at = pl.multiple_of(jnp.bitwise_xor(tp_ref[0], m) * tokens, 64)
-        values = comb_ref[m * tokens : (m + 1) * tokens] * column * gain
-        out_ref[pl.ds(at, tokens)] = values.astype(BF16)
+        copy = pltpu.make_async_copy(
+            held.at[pl.ds(m * tokens, tokens)], out_ref.at[pl.ds(at, tokens)], sent.at[m]
+        )
+        copy.start()
+        copies.append(copy)
+    for copy in copies:
+        copy.wait()
 
 
 def flip(value, axis, mask):
@@ -255,7 +290,7 @@
     )(*gather_all(shared_hidden, "tp"), sh_down)
 
     hidden = []
-    for g, blocks in enumerate(groups):
+    for blocks in groups:
         size = len(blocks)
         out = call(
             gated_kernel,
@@ -270,28 +305,42 @@
         for b, j in enumerate(blocks):
             block = out[b * capacity : (b + 1) * capacity]
             back.append(block if j == 0 else flip(block, "ep", j))
-        hidden += gather_all(jnp.concatenate(back, axis=0), "tp", steps=g < len(groups) - 1)
-
+        hidden += gather_all(jnp.concatenate(back, axis=0), "tp")
+
+    sizes, last = [len(blocks) for blocks in groups], experts - len(groups[-1])
+    sums_shape = shape((sources * rows, columns), F32)
+    slots, rest = last * capacity, sizes[-1] * capacity
+    sums = call(
+        functools.partial(early_kernel, sources, sizes[:-1], capacity),
+        sums_shape,
+        [VMEM] * (len(hidden) - sources + last + sources),
+        VMEM,
+        4 * sources * rows * slots * columns,
+        2 * last * inner * columns,
+        24,
+        [pltpu.VMEM((sources, slots, columns), BF16)],
+    )(*hidden[:-sources], *downs[:last], *metas)
     combined, squares = call(
-        functools.partial(combine_kernel, sources, [len(blocks) for blocks in groups], capacity),
-        [shape((sources * rows, columns), F32), shape((sources, rows), F32)],
-        [VMEM] * (len(hidden) + experts + sources + 1),
+        functools.partial(late_kernel, sources, sizes[-1], last, capacity),
+        [sums_shape, shape((sources, rows), F32)],
+        [VMEM] * (2 * sources + sizes[-1] + 2),
         [VMEM] * 2,
-        4 * sources * rows * experts * capacity * columns,
-        2 * experts * inner * columns,
+        4 * sources * rows * rest * columns,
+        2 * sizes[-1] * inner * columns,
         24,
-        [pltpu.VMEM((sources, experts * capacity, columns), BF16)],
-    )(*hidden, *downs, *metas, shared)
+        [pltpu.VMEM((sources, rest, columns), BF16)],
+    )(*hidden[-sources:], *downs[last:], *metas, shared, sums)
 
     gain = lax.dynamic_slice_in_dim(post_gain, tp[0] * columns, columns).reshape(1, columns)
     return call(
         functools.partial(final_kernel, width),
         shape((sources * rows, columns), BF16),
         [SMEM] + [VMEM] * (2 + sources),
-        VMEM,
+        HBM,
         8 * sources * rows * columns,
         6 * sources * rows * columns,
         16,
+        [pltpu.VMEM((sources * rows, columns), BF16), pltpu.SemaphoreType.DMA((sources,))],
     )(tp, combined, gain, *gather_all(squares, "tp", steps=False))
 
 

time: 186 us -> 191 us (1.027)
  waiting for transfers between devices: 99 us -> 119 us
  starting transfers between devices: 63 us -> 54.4 us
  local copies, waits for them, and re-layouts: 7.35 us -> 4.08 us
    ppermute x45, waiting for transfers between devices: 99 us -> 119 us  [flip(): return lax.ppermute(value, axis, [(i, i ^ mask) for i in range(size)])]
    ppermute x45, starting transfers between devices: 63 us -> 54.4 us  [flip(): return lax.ppermute(value, axis, [(i, i ^ mask) for i in range(size)])]
    unnamed x46 -> x26, local copies, waits for them, and re-layouts: 5.26 us -> 3.23 us
    pallas_call x8 -> x9, Pallas kernels: 14.8 us -> 13.6 us  [run(): pl.pallas_call(kernel, out_shape=out_shape, in_specs=in_specs, out_specs=...]
  transfers between devices with their start and end apart: 45 -> 45, of which waited for: 26 -> 20; matrix products, arithmetic and copies ran while one was open for 2% -> 0% of each run, Pallas kernels for 3% -> 3%
where the time goes in v2:
time: 191 us
  waiting for transfers between devices  119 us (62%)
  starting transfers between devices  54.4 us (28%)
  Pallas kernels  13.6 us (7%)
  local copies, waits for them, and re-layouts  4.08 us (2%)
    ppermute x45, waiting for transfers between devices, flip(): return lax.ppermute(value, axis, [(i, i ^ mask) for i in range(size)])  119 us
    ppermute x45, starting transfers between devices, flip(): return lax.ppermute(value, axis, [(i, i ^ mask) for i in range(size)])  54.4 us
    pallas_call x9, Pallas kernels, run(): pl.pallas_call(kernel, out_shape=out_shape, in_specs=in_specs, out_specs=...  13.6 us
  transfers between devices with their start and end apart: 45, of which 20 were waited for; matrix products, arithmetic and copies ran while one was open for 0% of the time, Pallas kernels for 3%

profile of v2, /device:TPU:0, one launch (start us, length us, event | category | flops | bytes accessed | tf_op | source)
XLA Modules:
  0.0 191.1 jit_solution(8812948215472870236)
XLA Ops:
  0.0 4.3 %shard_map.109 = (bf16[192,2048]{1,0:T(8,128)(2,1)}, f32[8,192]{1,0:T(8,128)}, bf16[64,2048]{1,0:T(8,128)(2,1)}, bf16[64,2048]{1,0:T(8,128)(2,1)}, bf16[64,2048]...) custom-call(s32[1]{0:T(128)} %bitcast.1.me_ref, ...), custom_call_target="tpu_custom_call" | custom-call | flops 402653184 | bytes 1572864 | tf_op jit(solution)/shard_map/pallas_call | solution.py:216
  4.3 4.1 %collective-permute-start.31 = (bf16[64,2048]{1,0:T(8,128)(2,1)}, bf16[64,2048]{1,0:T(8,128)(2,1)S(1)}, u32[]{:S(2)}, u32[]{:S(2)}) collective-permute-start(bf16[64,2048]{1,0:T(8,128)(2,1)} %get-tuple-element.25), channel_id=1, source_target_pairs={{0,16},{4,20},{8,24},{12,28},{16,0},{20,4},{24,8},{28,12},{1,17},{... | collective-permute-start | bytes 786440 | tf_op jit(solution)/shard_map/ppermute | solution.py:194
  8.5 1.3 collective-permute-start.32
  9.8 2.7 %collective-permute-start.7 = (bf16[512,512]{1,0:T(8,128)(2,1)S(1)}, bf16[512,512]{1,0:T(8,128)(2,1)S(1)}, u32[]{:S(2)}, u32[]{:S(2)}) collective-permute-start(bf16[512,512]{1,0:T(8,128)(2,1)S(1)} %dynamic-slice_bitcast_fusion.refs_8_), channel_id=1, source_target_pairs={{0,16},{4,20},{8,24},{12,28},{16,0},{20,4},{24,8},{28,12},{1,17},{... | collective-permute-start | bytes 1572872 | tf_op jit(solution)/shard_map/ppermute | solution.py:194
  12.4 1.6 collective-permute-start.39
  14.6 23.8 %collective-permute-done.31.refs_0_ = bf16[64,2048]{1,0:T(8,128)(2,1)S(1)} collective-permute-done((bf16[64,2048]{1,0:T(8,128)(2,1)}, bf16[64,2048]{1,0:T(8,128)(2,1)S(1)}, u32[]{:S(2)}, u32[]{:S(2)}) %collective-permute-start.31) | collective-permute-done | bytes 262176 | tf_op jit(solution)/shard_map/ppermute | solution.py:194
  38.4 6.9 %collective-permute-done.32.refs_1_ = bf16[64,2048]{1,0:T(8,128)(2,1)S(1)} collective-permute-done((bf16[64,2048]{1,0:T(8,128)(2,1)}, bf16[64,2048]{1,0:T(8,128)(2,1)S(1)}, u32[]{:S(2)}, u32[]{:S(2)}) %collective-permute-start.32) | collective-permute-done | bytes 262176 | tf_op jit(solution)/shard_map/ppermute | solution.py:194
  45.3 1.6 copy-done.1
  46.9 1.6 copy-done.3
  49.3 10.7 %collective-permute-done.23.refs_2_ = bf16[64,2048]{1,0:T(8,128)(2,1)S(1)} collective-permute-done((bf16[64,2048]{1,0:T(8,128)(2,1)}, bf16[64,2048]{1,0:T(8,128)(2,1)S(1)}, u32[]{:S(2)}, u32[]{:S(2)}) %collective-permute-start.23) | collective-permute-done | bytes 262176 | tf_op jit(solution)/shard_map/ppermute | solution.py:194
  60.0 3.5 %collective-permute-start = (bf16[64,2048]{1,0:T(8,128)(2,1)S(1)}, bf16[64,2048]{1,0:T(8,128)(2,1)S(1)}, u32[]{:S(2)}, u32[]{:S(2)}) collective-permute-start(bf16[64,2048]{1,0:T(8,128)(2,1)S(1)} %copy-done.11), channel_id=1, source_target_pairs={{0,24},{4,28},{8,16},{12,20},{16,8},{20,12},{24,0},{28,4},{1,25},{... | collective-permute-start | bytes 786440 | tf_op jit(solution)/shard_map/ppermute | solution.py:194
  63.6 8.6 %collective-permute-done.24.refs_3_ = bf16[64,2048]{1,0:T(8,128)(2,1)S(1)} collective-permute-done((bf16[64,2048]{1,0:T(8,128)(2,1)}, bf16[64,2048]{1,0:T(8,128)(2,1)S(1)}, u32[]{:S(2)}, u32[]{:S(2)}) %collective-permute-start.24) | collective-permute-done | bytes 262176 | tf_op jit(solution)/shard_map/ppermute | solution.py:194
  72.2 3.5 %collective-permute-start.1 = (bf16[64,2048]{1,0:T(8,128)(2,1)S(1)}, bf16[64,2048]{1,0:T(8,128)(2,1)S(1)}, u32[]{:S(2)}, u32[]{:S(2)}) collective-permute-start(bf16[64,2048]{1,0:T(8,128)(2,1)S(1)} %copy-done.10), channel_id=1, source_target_pairs={{0,28},{4,24},{8,20},{12,16},{16,12},{20,8},{24,4},{28,0},{1,29},{... | collective-permute-start | bytes 786440 | tf_op jit(solution)/shard_map/ppermute | solution.py:194
  75.6 1.2 shard_map.113
  76.9 1.6 collective-permute-start.11
  78.5 4.7 %collective-permute-done.1.refs_1_ = bf16[64,2048]{1,0:T(8,128)(2,1)S(1)} collective-permute-done((bf16[64,2048]{1,0:T(8,128)(2,1)S(1)}, bf16[64,2048]{1,0:T(8,128)(2,1)S(1)}, u32[]{:S(2)}, u32[]{:S(2)}) %collective-permute-start.1) | collective-permute-done | bytes 262176 | tf_op jit(solution)/shard_map/ppermute | solution.py:194
  83.2 4.5 %collective-permute-start.33 = (bf16[64,512]{1,0:T(8,128)(2,1)S(1)}, bf16[64,512]{1,0:T(8,128)(2,1)S(1)}, u32[]{:S(2)}, u32[]{:S(2)}) collective-permute-start(bf16[64,512]{1,0:T(8,128)(2,1)S(1)} %get-tuple-element.34), channel_id=1, source_target_pairs={{0,16},{4,20},{8,24},{12,28},{16,0},{20,4},{24,8},{28,12},{1,17},{... | collective-permute-start | bytes 196616 | tf_op jit(solution)/shard_map/ppermute | solution.py:194
  88.4 1.9 collective-permute-done.33
  90.3 2.3 %collective-permute-start.2 = (bf16[64,512]{1,0:T(8,128)(2,1)S(1)}, bf16[64,512]{1,0:T(8,128)(2,1)S(1)}, u32[]{:S(2)}, u32[]{:S(2)}) collective-permute-start(bf16[64,512]{1,0:T(8,128)(2,1)S(1)} %get-tuple-element.36), channel_id=1, source_target_pairs={{0,24},{4,28},{8,16},{12,20},{16,8},{20,12},{24,0},{28,4},{1,25},{... | collective-permute-start | bytes 196616 | tf_op jit(solution)/shard_map/ppermute | solution.py:194
  92.6 3.7 %collective-permute-done.2 = bf16[64,512]{1,0:T(8,128)(2,1)S(1)} collective-permute-done((bf16[64,512]{1,0:T(8,128)(2,1)S(1)}, bf16[64,512]{1,0:T(8,128)(2,1)S(1)}, u32[]{:S(2)}, u32[]{:S(2)}) %collective-permute-start.2) | collective-permute-done | bytes 65568 | tf_op jit(solution)/shard_map/ppermute | solution.py:194
  96.3 1.8 collective-permute-start.34
  98.2 1.2 collective-permute-start.25
  99.4 1.5 collective-permute-start.26
  100.8 1.9 collective-permute-done.34
  102.7 1.4 collective-permute-start.3
  104.0 1.5 collective-permute-start.27
  105.5 1.5 collective-permute-start.36
  107.0 2.7 %collective-permute-done.3 = bf16[64,512]{1,0:T(8,128)(2,1)S(1)} collective-permute-done((bf16[64,512]{1,0:T(8,128)(2,1)S(1)}, bf16[64,512]{1,0:T(8,128)(2,1)S(1)}, u32[]{:S(2)}, u32[]{:S(2)}) %collective-permute-start.3) | collective-permute-done | bytes 65568 | tf_op jit(solution)/shard_map/ppermute | solution.py:194
  110.0 1.7 collective-permute-start.5
  112.0 3.0 %collective-permute-start.38 = (bf16[512,512]{1,0:T(8,128)(2,1)S(1)}, bf16[512,512]{1,0:T(8,128)(2,1)S(1)}, u32[]{:S(2)}, u32[]{:S(2)}) collective-permute-start(bf16[512,512]{1,0:T(8,128)(2,1)S(1)} %dynamic-slice_bitcast_fusion.refs_8_), channel_id=1, source_target_pairs={{0,4},{4,0},{8,12},{12,8},{16,20},{20,16},{24,28},{28,24},{1,5},{5... | collective-permute-start | bytes 1572872 | tf_op jit(solution)/shard_map/ppermute | solution.py:194
  115.0 1.3 collective-permute-done.5.refs_2_
  116.4 1.7 collective-permute-start.17
  118.6 9.0 %collective-permute-done.14.refs_2_ = bf16[512,512]{1,0:T(8,128)(2,1)S(1)} collective-permute-done((bf16[512,512]{1,0:T(8,128)(2,1)S(1)}, bf16[512,512]{1,0:T(8,128)(2,1)S(1)}, u32[]{:S(2)}, u32[]{:S(2)}) %collective-permute-start.14) | collective-permute-done | bytes 524320 | tf_op jit(solution)/shard_map/ppermute | solution.py:194
  127.6 2.8 %collective-permute-start.8 = (bf16[512,512]{1,0:T(8,128)(2,1)S(1)}, bf16[512,512]{1,0:T(8,128)(2,1)S(1)}, u32[]{:S(2)}, u32[]{:S(2)}) collective-permute-start(bf16[512,512]{1,0:T(8,128)(2,1)S(1)} %collective-permute-done.7.refs_12_), channel_id=1, source_target_pairs={{0,8},{4,12},{8,0},{12,4},{16,24},{20,28},{24,16},{28,20},{1,9},{5... | collective-permute-start | bytes 1572872 | tf_op jit(solution)/shard_map/ppermute | solution.py:194
  130.4 7.9 %collective-permute-done.17.refs_6_ = bf16[512,512]{1,0:T(8,128)(2,1)S(1)} collective-permute-done((bf16[512,512]{1,0:T(8,128)(2,1)S(1)}, bf16[512,512]{1,0:T(8,128)(2,1)S(1)}, u32[]{:S(2)}, u32[]{:S(2)}) %collective-permute-start.17) | collective-permute-done | bytes 524320 | tf_op jit(solution)/shard_map/ppermute | solution.py:194
  138.3 1.8 collective-permute-start.29
  140.4 6.7 %collective-permute-done.29.refs_2_ = bf16[256,512]{1,0:T(8,128)(2,1)S(1)} collective-permute-done((bf16[256,512]{1,0:T(8,128)(2,1)S(1)}, bf16[256,512]{1,0:T(8,128)(2,1)S(1)}, u32[]{:S(2)}, u32[]{:S(2)}) %collective-permute-start.29) | collective-permute-done | bytes 262176 | tf_op jit(solution)/shard_map/ppermute | solution.py:194
  147.1 1.8 collective-permute-start.41
  149.2 1.8 collective-permute-start.9
  152.2 1.7 collective-permute-start.20
  154.0 5.4 %collective-permute-done.20.refs_2_ = bf16[192,512]{1,0:T(8,128)(2,1)S(1)} collective-permute-done((bf16[192,512]{1,0:T(8,128)(2,1)S(1)}, bf16[192,512]{1,0:T(8,128)(2,1)S(1)}, u32[]{:S(2)}, u32[]{:S(2)}) %collective-permute-start.20) | collective-permute-done | bytes 196640 | tf_op jit(solution)/shard_map/ppermute | solution.py:194
  159.4 2.5 %collective-permute-done.41.refs_13_ = bf16[512,512]{1,0:T(8,128)(2,1)S(1)} collective-permute-done((bf16[512,512]{1,0:T(8,128)(2,1)S(1)}, bf16[512,512]{1,0:T(8,128)(2,1)S(1)}, u32[]{:S(2)}, u32[]{:S(2)}) %collective-permute-start.41) | collective-permute-done | bytes 524320 | tf_op jit(solution)/shard_map/ppermute | solution.py:194
  161.9 11.2 %collective-permute-done.40.refs_11_ = bf16[512,512]{1,0:T(8,128)(2,1)S(1)} collective-permute-done((bf16[512,512]{1,0:T(8,128)(2,1)S(1)}, bf16[512,512]{1,0:T(8,128)(2,1)S(1)}, u32[]{:S(2)}, u32[]{:S(2)}) %collective-permute-start.40) | collective-permute-done | bytes 524320 | tf_op jit(solution)/shard_map/ppermute | solution.py:194
  173.2 1.9 shard_map.115.refs_11_
  175.7 7.4 %collective-permute-done.9.refs_5_ = bf16[512,512]{1,0:T(8,128)(2,1)S(1)} collective-permute-done((bf16[512,512]{1,0:T(8,128)(2,1)S(1)}, bf16[512,512]{1,0:T(8,128)(2,1)S(1)}, u32[]{:S(2)}, u32[]{:S(2)}) %collective-permute-start.9) | collective-permute-done | bytes 524320 | tf_op jit(solution)/shard_map/ppermute | solution.py:194
  183.1 1.9 %shard_map.116 = (f32[768,512]{1,0:T(8,128)S(1)}, f32[4,192]{1,0:T(4,128)S(1)}) custom-call(bf16[128,512]{1,0:T(8,128)(2,1)S(1)} %constant_dynamic-update-slice_fusion.refs_0_, bf16[128,512]{1,0:T(8,128)(2,1)S(1)} %collective-permute-done.4.refs_1_, bf16[128,512]{1,0:T(8,128)(2,1)S(1)} %collective-permute-done.5.refs_2_, ...), custom_call_target="tpu_custom_call" | custom-call | flops 201326592 | bytes 1048576 | tf_op jit(solution)/shard_map/pallas_call | solution.py:216
  185.1 1.8 collective-permute-start.43
  189.9 1.2 shard_map.117
  (85 shorter events, 8.9 us)
Async XLA Ops:
  4.3 34.0 %collective-permute-start.31 = (bf16[64,2048]{1,0:T(8,128)(2,1)}, bf16[64,2048]{1,0:T(8,128)(2,1)S(1)}, u32[]{:S(2)}, u32[]{:S(2)}) collective-permute-start(bf16[64,2048]{1,0:T(8,128)(2,1)} %get-tuple-element.25), channel_id=1, source_target_pairs={{0,16},{4,20},{8,24},{12,28},{16,0},{20,4},{24,8},{28,12},{1,17},{... | collective-permute-start | bytes 786440 | tf_op jit(solution)/shard_map/ppermute | solution.py:194
  8.5 36.8 %collective-permute-start.32 = (bf16[64,2048]{1,0:T(8,128)(2,1)}, bf16[64,2048]{1,0:T(8,128)(2,1)S(1)}, u32[]{:S(2)}, u32[]{:S(2)}) collective-permute-start(bf16[64,2048]{1,0:T(8,128)(2,1)} %get-tuple-element.26), channel_id=1, source_target_pairs={{0,20},{4,16},{8,28},{12,24},{16,4},{20,0},{24,12},{28,8},{1,21},{... | collective-permute-start | bytes 786440 | tf_op jit(solution)/shard_map/ppermute | solution.py:194
  9.8 108.3 %collective-permute-start.7 = (bf16[512,512]{1,0:T(8,128)(2,1)S(1)}, bf16[512,512]{1,0:T(8,128)(2,1)S(1)}, u32[]{:S(2)}, u32[]{:S(2)}) collective-permute-start(bf16[512,512]{1,0:T(8,128)(2,1)S(1)} %dynamic-slice_bitcast_fusion.refs_8_), channel_id=1, source_target_pairs={{0,16},{4,20},{8,24},{12,28},{16,0},{20,4},{24,8},{28,12},{1,17},{... | collective-permute-start | bytes 1572872 | tf_op jit(solution)/shard_map/ppermute | solution.py:194
  12.4 105.6 %collective-permute-start.39 = (bf16[512,512]{1,0:T(8,128)(2,1)S(1)}, bf16[512,512]{1,0:T(8,128)(2,1)S(1)}, u32[]{:S(2)}, u32[]{:S(2)}) collective-permute-start(bf16[512,512]{1,0:T(8,128)(2,1)S(1)} %dynamic-slice_bitcast_fusion.refs_8_), channel_id=1, source_target_pairs={{0,8},{4,12},{8,0},{12,4},{16,24},{20,28},{24,16},{28,20},{1,9},{5... | collective-permute-start | bytes 1572872 | tf_op jit(solution)/shard_map/ppermute | solution.py:194
  14.0 35.2 %collective-permute-start.22 = (bf16[64,2048]{1,0:T(8,128)(2,1)}, bf16[64,2048]{1,0:T(8,128)(2,1)S(1)}, u32[]{:S(2)}, u32[]{:S(2)}) collective-permute-start(bf16[64,2048]{1,0:T(8,128)(2,1)} %get-tuple-element.22), channel_id=1, source_target_pairs={{0,4},{4,0},{8,12},{12,8},{16,20},{20,16},{24,28},{28,24},{1,5},{5... | collective-permute-start | bytes 786440 | tf_op jit(solution)/shard_map/ppermute | solution.py:194
  38.3 21.7 %collective-permute-start.23 = (bf16[64,2048]{1,0:T(8,128)(2,1)}, bf16[64,2048]{1,0:T(8,128)(2,1)S(1)}, u32[]{:S(2)}, u32[]{:S(2)}) collective-permute-start(bf16[64,2048]{1,0:T(8,128)(2,1)} %get-tuple-element.23), channel_id=1, source_target_pairs={{0,8},{4,12},{8,0},{12,4},{16,24},{20,28},{24,16},{28,20},{1,9},{5... | collective-permute-start | bytes 786440 | tf_op jit(solution)/shard_map/ppermute | solution.py:194
  45.3 26.9 %collective-permute-start.24 = (bf16[64,2048]{1,0:T(8,128)(2,1)}, bf16[64,2048]{1,0:T(8,128)(2,1)S(1)}, u32[]{:S(2)}, u32[]{:S(2)}) collective-permute-start(bf16[64,2048]{1,0:T(8,128)(2,1)} %get-tuple-element.24), channel_id=1, source_target_pairs={{0,12},{4,8},{8,4},{12,0},{16,28},{20,24},{24,20},{28,16},{1,13},{... | collective-permute-start | bytes 786440 | tf_op jit(solution)/shard_map/ppermute | solution.py:194
  49.2 43.3 %collective-permute-start.10 = (f32[8,192]{1,0:T(8,128)S(1)}, f32[8,192]{1,0:T(8,128)S(1)}, u32[]{:S(2)}, u32[]{:S(2)}) collective-permute-start(f32[8,192]{1,0:T(8,128)S(1)} %copy-done.9), channel_id=1, source_target_pairs={{0,1},{1,0},{2,3},{3,2},{4,5},{5,4},{6,7},{7,6},{8,9},{9,8},{10,11... | collective-permute-start | bytes 18440 | tf_op jit(solution)/shard_map/ppermute | solution.py:194
  60.0 16.9 %collective-permute-start = (bf16[64,2048]{1,0:T(8,128)(2,1)S(1)}, bf16[64,2048]{1,0:T(8,128)(2,1)S(1)}, u32[]{:S(2)}, u32[]{:S(2)}) collective-permute-start(bf16[64,2048]{1,0:T(8,128)(2,1)S(1)} %copy-done.11), channel_id=1, source_target_pairs={{0,24},{4,28},{8,16},{12,20},{16,8},{20,12},{24,0},{28,4},{1,25},{... | collective-permute-start | bytes 786440 | tf_op jit(solution)/shard_map/ppermute | solution.py:194
  72.2 11.0 %collective-permute-start.1 = (bf16[64,2048]{1,0:T(8,128)(2,1)S(1)}, bf16[64,2048]{1,0:T(8,128)(2,1)S(1)}, u32[]{:S(2)}, u32[]{:S(2)}) collective-permute-start(bf16[64,2048]{1,0:T(8,128)(2,1)S(1)} %copy-done.10), channel_id=1, source_target_pairs={{0,28},{4,24},{8,20},{12,16},{16,12},{20,8},{24,4},{28,0},{1,29},{... | collective-permute-start | bytes 786440 | tf_op jit(solution)/shard_map/ppermute | solution.py:194
  76.9 21.3 %collective-permute-start.11 = (f32[8,192]{1,0:T(8,128)S(1)}, f32[8,192]{1,0:T(8,128)S(1)}, u32[]{:S(2)}, u32[]{:S(2)}) collective-permute-start(f32[8,192]{1,0:T(8,128)S(1)} %copy-done.9), channel_id=1, source_target_pairs={{0,2},{1,3},{2,0},{3,1},{4,6},{5,7},{6,4},{7,5},{8,10},{9,11},{10,... | collective-permute-start | bytes 18440 | tf_op jit(solution)/shard_map/ppermute | solution.py:194
  83.2 28.5 %copy-start.6 = (bf16[512,512]{1,0:T(8,128)(2,1)S(1)}, bf16[512,512]{1,0:T(8,128)(2,1)}, u32[]{:S(2)}) copy-start(bf16[512,512]{1,0:T(8,128)(2,1)} %refs_0_.1) | copy-start | bytes 1572868
  83.2 33.2 %copy-start.7 = (bf16[512,512]{1,0:T(8,128)(2,1)S(1)}, bf16[512,512]{1,0:T(8,128)(2,1)}, u32[]{:S(2)}) copy-start(bf16[512,512]{1,0:T(8,128)(2,1)} %refs_4_.3) | copy-start | bytes 1572868
  83.2 68.0 %copy-start.4 = (bf16[192,2048]{1,0:T(8,128)(2,1)S(1)}, bf16[192,2048]{1,0:T(8,128)(2,1)}, u32[]{:S(2)}) copy-start(bf16[192,2048]{1,0:T(8,128)(2,1)} %get-tuple-element.20.normed_ref) | copy-start | bytes 2359300
  83.2 7.1 %collective-permute-start.33 = (bf16[64,512]{1,0:T(8,128)(2,1)S(1)}, bf16[64,512]{1,0:T(8,128)(2,1)S(1)}, u32[]{:S(2)}, u32[]{:S(2)}) collective-permute-start(bf16[64,512]{1,0:T(8,128)(2,1)S(1)} %get-tuple-element.34), channel_id=1, source_target_pairs={{0,16},{4,20},{8,24},{12,28},{16,0},{20,4},{24,8},{28,12},{1,17},{... | collective-permute-start | bytes 196616 | tf_op jit(solution)/shard_map/ppermute | solution.py:194
  90.3 6.1 %collective-permute-start.2 = (bf16[64,512]{1,0:T(8,128)(2,1)S(1)}, bf16[64,512]{1,0:T(8,128)(2,1)S(1)}, u32[]{:S(2)}, u32[]{:S(2)}) collective-permute-start(bf16[64,512]{1,0:T(8,128)(2,1)S(1)} %get-tuple-element.36), channel_id=1, source_target_pairs={{0,24},{4,28},{8,16},{12,20},{16,8},{20,12},{24,0},{28,4},{1,25},{... | collective-permute-start | bytes 196616 | tf_op jit(solution)/shard_map/ppermute | solution.py:194
  92.6 6.8 %collective-permute-start.12 = (f32[8,192]{1,0:T(8,128)S(1)}, f32[8,192]{1,0:T(8,128)S(1)}, u32[]{:S(2)}, u32[]{:S(2)}) collective-permute-start(f32[8,192]{1,0:T(8,128)S(1)} %copy-done.9), channel_id=1, source_target_pairs={{0,3},{1,2},{2,1},{3,0},{4,7},{5,6},{6,5},{7,4},{8,11},{9,10},{10,... | collective-permute-start | bytes 18440 | tf_op jit(solution)/shard_map/ppermute | solution.py:194
  96.3 6.3 %collective-permute-start.34 = (bf16[64,512]{1,0:T(8,128)(2,1)S(1)}, bf16[64,512]{1,0:T(8,128)(2,1)S(1)}, u32[]{:S(2)}, u32[]{:S(2)}) collective-permute-start(bf16[64,512]{1,0:T(8,128)(2,1)S(1)} %get-tuple-element.33), channel_id=1, source_target_pairs={{0,20},{4,16},{8,28},{12,24},{16,4},{20,0},{24,12},{28,8},{1,21},{... | collective-permute-start | bytes 196616 | tf_op jit(solution)/shard_map/ppermute | solution.py:194
  98.2 5.9 %collective-permute-start.25 = (bf16[64,512]{1,0:T(8,128)(2,1)S(1)}, bf16[64,512]{1,0:T(8,128)(2,1)S(1)}, u32[]{:S(2)}, u32[]{:S(2)}) collective-permute-start(bf16[64,512]{1,0:T(8,128)(2,1)S(1)} %get-tuple-element.32), channel_id=1, source_target_pairs={{0,4},{4,0},{8,12},{12,8},{16,20},{20,16},{24,28},{28,24},{1,5},{5... | collective-permute-start | bytes 196616 | tf_op jit(solution)/shard_map/ppermute | solution.py:194
  99.4 6.2 %collective-permute-start.26 = (bf16[64,512]{1,0:T(8,128)(2,1)S(1)}, bf16[64,512]{1,0:T(8,128)(2,1)S(1)}, u32[]{:S(2)}, u32[]{:S(2)}) collective-permute-start(bf16[64,512]{1,0:T(8,128)(2,1)S(1)} %get-tuple-element.31), channel_id=1, source_target_pairs={{0,8},{4,12},{8,0},{12,4},{16,24},{20,28},{24,16},{28,20},{1,9},{5... | collective-permute-start | bytes 196616 | tf_op jit(solution)/shard_map/ppermute | solution.py:194
  102.7 7.1 %collective-permute-start.3 = (bf16[64,512]{1,0:T(8,128)(2,1)S(1)}, bf16[64,512]{1,0:T(8,128)(2,1)S(1)}, u32[]{:S(2)}, u32[]{:S(2)}) collective-permute-start(bf16[64,512]{1,0:T(8,128)(2,1)S(1)} %get-tuple-element.35), channel_id=1, source_target_pairs={{0,28},{4,24},{8,20},{12,16},{16,12},{20,8},{24,4},{28,0},{1,29},{... | collective-permute-start | bytes 196616 | tf_op jit(solution)/shard_map/ppermute | solution.py:194
  104.0 5.9 %collective-permute-start.27 = (bf16[64,512]{1,0:T(8,128)(2,1)S(1)}, bf16[64,512]{1,0:T(8,128)(2,1)S(1)}, u32[]{:S(2)}, u32[]{:S(2)}) collective-permute-start(bf16[64,512]{1,0:T(8,128)(2,1)S(1)} %get-tuple-element.30), channel_id=1, source_target_pairs={{0,12},{4,8},{8,4},{12,0},{16,28},{20,24},{24,20},{28,16},{1,13},{... | collective-permute-start | bytes 196616 | tf_op jit(solution)/shard_map/ppermute | solution.py:194
  105.5 6.2 %collective-permute-start.36 = (bf16[128,512]{1,0:T(8,128)(2,1)S(1)}, bf16[128,512]{1,0:T(8,128)(2,1)S(1)}, u32[]{:S(2)}, u32[]{:S(2)}) collective-permute-start(bf16[128,512]{1,0:T(8,128)(2,1)S(1)} %constant_dynamic-update-slice_fusion.2.refs_4_), channel_id=1, source_target_pairs={{0,2},{1,3},{2,0},{3,1},{4,6},{5,7},{6,4},{7,5},{8,10},{9,11},{10,... | collective-permute-start | bytes 393224 | tf_op jit(solution)/shard_map/ppermute | solution.py:194
  109.7 2.3 %collective-permute-start.35 = (bf16[128,512]{1,0:T(8,128)(2,1)S(1)}, bf16[128,512]{1,0:T(8,128)(2,1)S(1)}, u32[]{:S(2)}, u32[]{:S(2)}) collective-permute-start(bf16[128,512]{1,0:T(8,128)(2,1)S(1)} %constant_dynamic-update-slice_fusion.2.refs_4_), channel_id=1, source_target_pairs={{0,1},{1,0},{2,3},{3,2},{4,5},{5,4},{6,7},{7,6},{8,9},{9,8},{10,11... | collective-permute-start | bytes 393224 | tf_op jit(solution)/shard_map/ppermute | solution.py:194
  110.0 6.4 %collective-permute-start.5 = (bf16[128,512]{1,0:T(8,128)(2,1)S(1)}, bf16[128,512]{1,0:T(8,128)(2,1)S(1)}, u32[]{:S(2)}, u32[]{:S(2)}) collective-permute-start(bf16[128,512]{1,0:T(8,128)(2,1)S(1)} %constant_dynamic-update-slice_fusion.refs_0_), channel_id=1, source_target_pairs={{0,2},{1,3},{2,0},{3,1},{4,6},{5,7},{6,4},{7,5},{8,10},{9,11},{10,... | collective-permute-start | bytes 393224 | tf_op jit(solution)/shard_map/ppermute | solution.py:194
  111.7 15.9 %collective-permute-start.14 = (bf16[512,512]{1,0:T(8,128)(2,1)S(1)}, bf16[512,512]{1,0:T(8,128)(2,1)S(1)}, u32[]{:S(2)}, u32[]{:S(2)}) collective-permute-start(bf16[512,512]{1,0:T(8,128)(2,1)S(1)} %copy-done.6), channel_id=1, source_target_pairs={{0,2},{1,3},{2,0},{3,1},{4,6},{5,7},{6,4},{7,5},{8,10},{9,11},{10,... | collective-permute-start | bytes 1572872 | tf_op jit(solution)/shard_map/ppermute | solution.py:194
  112.0 15.6 %collective-permute-start.38 = (bf16[512,512]{1,0:T(8,128)(2,1)S(1)}, bf16[512,512]{1,0:T(8,128)(2,1)S(1)}, u32[]{:S(2)}, u32[]{:S(2)}) collective-permute-start(bf16[512,512]{1,0:T(8,128)(2,1)S(1)} %dynamic-slice_bitcast_fusion.refs_8_), channel_id=1, source_target_pairs={{0,4},{4,0},{8,12},{12,8},{16,20},{20,16},{24,28},{28,24},{1,5},{5... | collective-permute-start | bytes 1572872 | tf_op jit(solution)/shard_map/ppermute | solution.py:194
  116.4 22.0 %collective-permute-start.17 = (bf16[512,512]{1,0:T(8,128)(2,1)S(1)}, bf16[512,512]{1,0:T(8,128)(2,1)S(1)}, u32[]{:S(2)}, u32[]{:S(2)}) collective-permute-start(bf16[512,512]{1,0:T(8,128)(2,1)S(1)} %copy-done.7), channel_id=1, source_target_pairs={{0,2},{1,3},{2,0},{3,1},{4,6},{5,7},{6,4},{7,5},{8,10},{9,11},{10,... | collective-permute-start | bytes 1572872 | tf_op jit(solution)/shard_map/ppermute | solution.py:194
  118.1 20.3 %collective-permute-start.13 = (bf16[512,512]{1,0:T(8,128)(2,1)S(1)}, bf16[512,512]{1,0:T(8,128)(2,1)S(1)}, u32[]{:S(2)}, u32[]{:S(2)}) collective-permute-start(bf16[512,512]{1,0:T(8,128)(2,1)S(1)} %copy-done.6), channel_id=1, source_target_pairs={{0,1},{1,0},{2,3},{3,2},{4,5},{5,4},{6,7},{7,6},{8,9},{9,8},{10,11... | collective-permute-start | bytes 1572872 | tf_op jit(solution)/shard_map/ppermute | solution.py:194
  118.1 22.1 %collective-permute-start.16 = (bf16[512,512]{1,0:T(8,128)(2,1)S(1)}, bf16[512,512]{1,0:T(8,128)(2,1)S(1)}, u32[]{:S(2)}, u32[]{:S(2)}) collective-permute-start(bf16[512,512]{1,0:T(8,128)(2,1)S(1)} %copy-done.7), channel_id=1, source_target_pairs={{0,1},{1,0},{2,3},{3,2},{4,5},{5,4},{6,7},{7,6},{8,9},{9,8},{10,11... | collective-permute-start | bytes 1572872 | tf_op jit(solution)/shard_map/ppermute | solution.py:194
  127.6 21.6 %collective-permute-start.15 = (bf16[512,512]{1,0:T(8,128)(2,1)S(1)}, bf16[512,512]{1,0:T(8,128)(2,1)S(1)}, u32[]{:S(2)}, u32[]{:S(2)}) collective-permute-start(bf16[512,512]{1,0:T(8,128)(2,1)S(1)} %collective-permute-done.14.refs_2_), channel_id=1, source_target_pairs={{0,1},{1,0},{2,3},{3,2},{4,5},{5,4},{6,7},{7,6},{8,9},{9,8},{10,11... | collective-permute-start | bytes 1572872 | tf_op jit(solution)/shard_map/ppermute | solution.py:194
  127.6 21.6 %collective-permute-start.8 = (bf16[512,512]{1,0:T(8,128)(2,1)S(1)}, bf16[512,512]{1,0:T(8,128)(2,1)S(1)}, u32[]{:S(2)}, u32[]{:S(2)}) collective-permute-start(bf16[512,512]{1,0:T(8,128)(2,1)S(1)} %collective-permute-done.7.refs_12_), channel_id=1, source_target_pairs={{0,8},{4,12},{8,0},{12,4},{16,24},{20,28},{24,16},{28,20},{1,9},{5... | collective-permute-start | bytes 1572872 | tf_op jit(solution)/shard_map/ppermute | solution.py:194
  138.3 12.7 %collective-permute-start.18 = (bf16[512,512]{1,0:T(8,128)(2,1)S(1)}, bf16[512,512]{1,0:T(8,128)(2,1)S(1)}, u32[]{:S(2)}, u32[]{:S(2)}) collective-permute-start(bf16[512,512]{1,0:T(8,128)(2,1)S(1)} %collective-permute-done.17.refs_6_), channel_id=1, source_target_pairs={{0,1},{1,0},{2,3},{3,2},{4,5},{5,4},{6,7},{7,6},{8,9},{9,8},{10,11... | collective-permute-start | bytes 1572872 | tf_op jit(solution)/shard_map/ppermute | solution.py:194
  138.3 8.8 %collective-permute-start.29 = (bf16[256,512]{1,0:T(8,128)(2,1)S(1)}, bf16[256,512]{1,0:T(8,128)(2,1)S(1)}, u32[]{:S(2)}, u32[]{:S(2)}) collective-permute-start(bf16[256,512]{1,0:T(8,128)(2,1)S(1)} %pad_maximum_fusion.refs_0_), channel_id=1, source_target_pairs={{0,2},{1,3},{2,0},{3,1},{4,6},{5,7},{6,4},{7,5},{8,10},{9,11},{10,... | collective-permute-start | bytes 786440 | tf_op jit(solution)/shard_map/ppermute | solution.py:194
  140.2 8.7 %collective-permute-start.28 = (bf16[256,512]{1,0:T(8,128)(2,1)S(1)}, bf16[256,512]{1,0:T(8,128)(2,1)S(1)}, u32[]{:S(2)}, u32[]{:S(2)}) collective-permute-start(bf16[256,512]{1,0:T(8,128)(2,1)S(1)} %pad_maximum_fusion.refs_0_), channel_id=1, source_target_pairs={{0,1},{1,0},{2,3},{3,2},{4,5},{5,4},{6,7},{7,6},{8,9},{9,8},{10,11... | collective-permute-start | bytes 786440 | tf_op jit(solution)/shard_map/ppermute | solution.py:194
  147.1 14.8 %collective-permute-start.41 = (bf16[512,512]{1,0:T(8,128)(2,1)S(1)}, bf16[512,512]{1,0:T(8,128)(2,1)S(1)}, u32[]{:S(2)}, u32[]{:S(2)}) collective-permute-start(bf16[512,512]{1,0:T(8,128)(2,1)S(1)} %collective-permute-done.7.refs_12_), channel_id=1, source_target_pairs={{0,4},{4,0},{8,12},{12,8},{16,20},{20,16},{24,28},{28,24},{1,5},{5... | collective-permute-start | bytes 1572872 | tf_op jit(solution)/shard_map/ppermute | solution.py:194
  148.9 24.3 %collective-permute-start.40 = (bf16[512,512]{1,0:T(8,128)(2,1)S(1)}, bf16[512,512]{1,0:T(8,128)(2,1)S(1)}, u32[]{:S(2)}, u32[]{:S(2)}) collective-permute-start(bf16[512,512]{1,0:T(8,128)(2,1)S(1)} %collective-permute-done.39.refs_10_), channel_id=1, source_target_pairs={{0,4},{4,0},{8,12},{12,8},{16,20},{20,16},{24,28},{28,24},{1,5},{5... | collective-permute-start | bytes 1572872 | tf_op jit(solution)/shard_map/ppermute | solution.py:194
  149.2 3.0 %collective-permute-start.37 = (bf16[128,512]{1,0:T(8,128)(2,1)S(1)}, bf16[128,512]{1,0:T(8,128)(2,1)S(1)}, u32[]{:S(2)}, u32[]{:S(2)}) collective-permute-start(bf16[128,512]{1,0:T(8,128)(2,1)S(1)} %collective-permute-done.36.refs_6_), channel_id=1, source_target_pairs={{0,1},{1,0},{2,3},{3,2},{4,5},{5,4},{6,7},{7,6},{8,9},{9,8},{10,11... | collective-permute-start | bytes 393224 | tf_op jit(solution)/shard_map/ppermute | solution.py:194
  149.2 33.9 %collective-permute-start.9 = (bf16[512,512]{1,0:T(8,128)(2,1)S(1)}, bf16[512,512]{1,0:T(8,128)(2,1)S(1)}, u32[]{:S(2)}, u32[]{:S(2)}) collective-permute-start(bf16[512,512]{1,0:T(8,128)(2,1)S(1)} %collective-permute-done.8.refs_4_), channel_id=1, source_target_pairs={{0,4},{4,0},{8,12},{12,8},{16,20},{20,16},{24,28},{28,24},{1,5},{5... | collective-permute-start | bytes 1572872 | tf_op jit(solution)/shard_map/ppermute | solution.py:194
  151.0 2.9 %collective-permute-start.30 = (bf16[256,512]{1,0:T(8,128)(2,1)S(1)}, bf16[256,512]{1,0:T(8,128)(2,1)S(1)}, u32[]{:S(2)}, u32[]{:S(2)}) collective-permute-start(bf16[256,512]{1,0:T(8,128)(2,1)S(1)} %collective-permute-done.29.refs_2_), channel_id=1, source_target_pairs={{0,1},{1,0},{2,3},{3,2},{4,5},{5,4},{6,7},{7,6},{8,9},{9,8},{10,11... | collective-permute-start | bytes 786440 | tf_op jit(solution)/shard_map/ppermute | solution.py:194
  152.2 7.2 %collective-permute-start.20 = (bf16[192,512]{1,0:T(8,128)(2,1)S(1)}, bf16[192,512]{1,0:T(8,128)(2,1)S(1)}, u32[]{:S(2)}, u32[]{:S(2)}) collective-permute-start(bf16[192,512]{1,0:T(8,128)(2,1)S(1)} %shard_map.111.refs_0_), channel_id=1, source_target_pairs={{0,2},{1,3},{2,0},{3,1},{4,6},{5,7},{6,4},{7,5},{8,10},{9,11},{10,... | collective-permute-start | bytes 589832 | tf_op jit(solution)/shard_map/ppermute | solution.py:194
  154.0 21.1 %collective-permute-start.19 = (bf16[192,512]{1,0:T(8,128)(2,1)S(1)}, bf16[192,512]{1,0:T(8,128)(2,1)S(1)}, u32[]{:S(2)}, u32[]{:S(2)}) collective-permute-start(bf16[192,512]{1,0:T(8,128)(2,1)S(1)} %shard_map.111.refs_0_), channel_id=1, source_target_pairs={{0,1},{1,0},{2,3},{3,2},{4,5},{5,4},{6,7},{7,6},{8,9},{9,8},{10,11... | collective-permute-start | bytes 589832 | tf_op jit(solution)/shard_map/ppermute | solution.py:194
  159.4 15.6 %collective-permute-start.21 = (bf16[192,512]{1,0:T(8,128)(2,1)S(1)}, bf16[192,512]{1,0:T(8,128)(2,1)S(1)}, u32[]{:S(2)}, u32[]{:S(2)}) collective-permute-start(bf16[192,512]{1,0:T(8,128)(2,1)S(1)} %collective-permute-done.20.refs_2_), channel_id=1, source_target_pairs={{0,1},{1,0},{2,3},{3,2},{4,5},{5,4},{6,7},{7,6},{8,9},{9,8},{10,11... | collective-permute-start | bytes 589832 | tf_op jit(solution)/shard_map/ppermute | solution.py:194
  161.9 13.7 %collective-permute-start.4 = (bf16[128,512]{1,0:T(8,128)(2,1)S(1)}, bf16[128,512]{1,0:T(8,128)(2,1)S(1)}, u32[]{:S(2)}, u32[]{:S(2)}) collective-permute-start(bf16[128,512]{1,0:T(8,128)(2,1)S(1)} %constant_dynamic-update-slice_fusion.refs_0_), channel_id=1, source_target_pairs={{0,1},{1,0},{2,3},{3,2},{4,5},{5,4},{6,7},{7,6},{8,9},{9,8},{10,11... | collective-permute-start | bytes 393224 | tf_op jit(solution)/shard_map/ppermute | solution.py:194
  173.2 2.5 %collective-permute-start.6 = (bf16[128,512]{1,0:T(8,128)(2,1)S(1)}, bf16[128,512]{1,0:T(8,128)(2,1)S(1)}, u32[]{:S(2)}, u32[]{:S(2)}) collective-permute-start(bf16[128,512]{1,0:T(8,128)(2,1)S(1)} %collective-permute-done.5.refs_2_), channel_id=1, source_target_pairs={{0,1},{1,0},{2,3},{3,2},{4,5},{5,4},{6,7},{7,6},{8,9},{9,8},{10,11... | collective-permute-start | bytes 393224 | tf_op jit(solution)/shard_map/ppermute | solution.py:194
  185.0 2.7 %collective-permute-start.42 = (f32[4,192]{1,0:T(4,128)S(1)}, f32[4,192]{1,0:T(4,128)S(1)}, u32[]{:S(2)}, u32[]{:S(2)}) collective-permute-start(f32[4,192]{1,0:T(4,128)S(1)} %get-tuple-element.28.refs_0_), channel_id=1, source_target_pairs={{0,1},{1,0},{2,3},{3,2},{4,5},{5,4},{6,7},{7,6},{8,9},{9,8},{10,11... | collective-permute-start | bytes 9224 | tf_op jit(solution)/shard_map/ppermute | solution.py:194
  185.1 3.7 %collective-permute-start.43 = (f32[4,192]{1,0:T(4,128)S(1)}, f32[4,192]{1,0:T(4,128)S(1)}, u32[]{:S(2)}, u32[]{:S(2)}) collective-permute-start(f32[4,192]{1,0:T(4,128)S(1)} %get-tuple-element.28.refs_0_), channel_id=1, source_target_pairs={{0,2},{1,3},{2,0},{3,1},{4,6},{5,7},{6,4},{7,5},{8,10},{9,11},{10,... | collective-permute-start | bytes 9224 | tf_op jit(solution)/shard_map/ppermute | solution.py:194
  186.9 3.0 %collective-permute-start.44 = (f32[4,192]{1,0:T(4,128)S(1)}, f32[4,192]{1,0:T(4,128)S(1)}, u32[]{:S(2)}, u32[]{:S(2)}) collective-permute-start(f32[4,192]{1,0:T(4,128)S(1)} %get-tuple-element.28.refs_0_), channel_id=1, source_target_pairs={{0,3},{1,2},{2,1},{3,0},{4,7},{5,6},{6,5},{7,4},{8,11},{9,10},{10,... | collective-permute-start | bytes 9224 | tf_op jit(solution)/shard_map/ppermute | solution.py:194
  (9 other events, 126.1 us)
